TPU v7x, 128 devices: a whole 4x4x4 slice. The times are simulated.
128 devices in a mesh: ep: 64 (over z, y, x), tp: 2 (over core).
Axes of the slice: x: 4, y: 4, z: 4, core: 2. Of those that a mesh axis runs over, the one named last changes fastest.
Arguments:
- tokens: bfloat16 [3072, 2048], P('ep'), may hold values from -6 to 6
- norm_gain: bfloat16 [2048], replicated, as said below
- expert_gain: bfloat16 [2048], replicated, may hold values from 0.099609375 to 1.8984375
- w_query: bfloat16 [2048, 512], P(None, 'tp'), as said below
- key_weight: bfloat16 [2048, 256], P(None, 'tp'), may hold values from -0.125 to 0.125
- value_weight: bfloat16 [2048, 256], P(None, 'tp'), may hold values from -0.125 to 0.125
- forget_weight: bfloat16 [2048, 2], replicated, may hold values from -0.125 to 0.125
- w_out: bfloat16 [512, 2048], P('tp'), may hold values from -0.25 to 0.25
- key_cache: bfloat16 [3072, 1024, 2, 128], P('ep', None, 'tp'), may hold values from -64 to 64
- cached_values: bfloat16 [3072, 1024, 2, 128], P('ep', None, 'tp'), may hold values from -6 to 6
- cum_gates: float32 [3072, 2, 1024], P('ep', 'tp'), as said below
- lengths: int32 [3072], P('ep'), may hold values from 128 to 1024
- routes: int32 [3072, 4], P('ep'), may hold values from 0 to 63, all different within a row; in each aligned block of 48 rows (0 to 47, 48 to 95, ...) at most 6 rows name the same one
- route_weights: float32 [3072, 4], P('ep'), may hold values from 0.1 to 1
- expert_gate: bfloat16 [64, 2048, 512], P('ep', None, 'tp'), may hold values from -0.125 to 0.125
- expert_up: bfloat16 [64, 2048, 512], P('ep', None, 'tp'), may hold values from -0.125 to 0.125
- expert_down: bfloat16 [64, 512, 2048], P('ep', 'tp'), may hold values from -0.25 to 0.25
Outputs:
- hidden_out: bfloat16 [3072, 2048], P('ep', 'tp')
Inputs may be any that keep to these rules, and one draw needn't show every extreme that they name: `routes`: each row names 4 different experts. Among the 48 rows of one index of ep no expert is named more than 6 times, a bound that some block reaches. `cum_gates`: entry p is the sum of the log forget values of positions 0 to p, so it never rises along the last dimension. `norm_gain`: every entry is positive and of order one. `w_query`: entries have mean zero and a spread of one over the square root of 2048.
All inputs are finite; a program needn't handle non-finite values.
Results may differ from a plain program's by a relative error of at most 0.014.
Values may be sent and summed in bfloat16 or wider, within the bound.
No kernel may reach another device: no remote copies, remote signals or barrier semaphores. Data moves between devices by JAX's collectives and lax.ppermute only.
A program may use at most 128 MiB of HBM per device.

v0:
```python
import jax
import jax.numpy as jnp
from jax import lax
from jax.sharding import PartitionSpec as P

EPS = 1e-06


def sent_to_all(array, axis):
    size = lax.axis_size(axis)
    return lax.all_to_all(
        jnp.broadcast_to(array[None], (size, *array.shape)), axis, 0, 0, tiled=True
    )


def of_everyone(array, axis):
    return sent_to_all(array, axis).astype(jnp.float32).sum(axis=0)


def cut_along(array, dim, size):
    before, after = (array.shape[:dim], array.shape[dim + 1 :])
    return jnp.moveaxis(array.reshape(*before, size, -1, *after), dim, 0)


def sent_and_summed(array, axis, dim):
    blocks = cut_along(array, dim, lax.axis_size(axis))
    arrived = lax.all_to_all(blocks, axis, split_axis=0, concat_axis=0, tiled=True)
    return arrived.astype(jnp.float32).sum(axis=0)


def rms_rows(values, gain):
    flt = values.astype(jnp.float32)
    scale = lax.rsqrt(jnp.mean(flt * flt, axis=-1, keepdims=True) + EPS)
    return (flt * scale * gain.astype(jnp.float32)).astype(jnp.bfloat16)


def attend(
    query_rows, key_new, value_new, log_forget, key_cache, cached_values, cum_gates, lengths
):
    seqs = key_cache.shape[0]
    kv_heads = key_cache.shape[2]
    head_size = key_cache.shape[3]
    group = query_rows.shape[1] // (kv_heads * head_size)
    scale = head_size ** (-0.5)
    q_four = query_rows.reshape(seqs, kv_heads, group, head_size)
    k_self = key_new.reshape(seqs, kv_heads, head_size)
    v_self = value_new.reshape(seqs, kv_heads, head_size)
    places = jnp.arange(key_cache.shape[1], dtype=jnp.int32)
    last = jnp.sum(
        jnp.where(places[None, None, :] == (lengths - 1)[:, None, None], cum_gates, 0.0), axis=-1
    )
    bias = (log_forget + last)[:, :, None] - cum_gates
    scores = (
        jnp.einsum("skgd,slkd->skgl", q_four, key_cache, preferred_element_type=jnp.float32) * scale
    )
    scores = scores + bias[:, :, None, :]
    valid = places[None, :] < lengths[:, None]
    scores = jnp.where(valid[:, None, None, :], scores, -jnp.inf)
    own = jnp.einsum("skgd,skd->skg", q_four, k_self, preferred_element_type=jnp.float32) * scale
    top = jnp.maximum(jnp.max(scores, axis=-1), own)
    expo = jnp.exp(scores - top[..., None])
    own_expo = jnp.exp(own - top)
    denom = jnp.sum(expo, axis=-1) + own_expo
    probs = (expo / denom[..., None]).astype(jnp.bfloat16)
    own_prob = (own_expo / denom).astype(jnp.bfloat16)
    result = jnp.einsum("skgl,slkd->skgd", probs, cached_values, preferred_element_type=jnp.float32)
    result = (
        result + own_prob.astype(jnp.float32)[..., None] * v_self.astype(jnp.float32)[:, :, None, :]
    )
    return result.astype(jnp.bfloat16).reshape(seqs, kv_heads * group * head_size)


def expert_ffn(received, gate_w, up_w, down_w):
    gate = jnp.einsum("necd,edf->necf", received, gate_w, preferred_element_type=jnp.float32)
    upper = jnp.einsum("necd,edf->necf", received, up_w, preferred_element_type=jnp.float32)
    act = (jax.nn.silu(gate) * upper).astype(jnp.bfloat16)
    return jnp.einsum("necf,efd->necd", act, down_w, preferred_element_type=jnp.float32)


def shards(
    tokens,
    norm_gain,
    expert_gain,
    w_query,
    key_weight,
    value_weight,
    forget_weight,
    w_out,
    key_cache,
    cached_values,
    cum_gates,
    lengths,
    routes,
    route_weights,
    expert_gate,
    expert_up,
    expert_down,
):
    seqs, width = tokens.shape
    n_ep = lax.axis_size("ep")
    kv_loc = key_cache.shape[2]
    normed = rms_rows(tokens, norm_gain)
    forget_cols = lax.dynamic_slice_in_dim(forget_weight, lax.axis_index("tp") * kv_loc, kv_loc, 1)
    log_forget = jax.nn.log_sigmoid(
        jnp.dot(normed, forget_cols, preferred_element_type=jnp.float32)
    )
    query_rows = jnp.dot(normed, w_query, preferred_element_type=jnp.float32).astype(jnp.bfloat16)
    key_new = jnp.dot(normed, key_weight, preferred_element_type=jnp.float32).astype(jnp.bfloat16)
    value_new = jnp.dot(normed, value_weight, preferred_element_type=jnp.float32).astype(
        jnp.bfloat16
    )
    attended = attend(
        query_rows, key_new, value_new, log_forget, key_cache, cached_values, cum_gates, lengths
    )
    partial_out = jnp.dot(attended, w_out, preferred_element_type=jnp.float32)
    mixed = of_everyone(partial_out.astype(jnp.bfloat16), "tp").astype(jnp.float32)
    resid = (tokens.astype(jnp.float32) + mixed).astype(jnp.bfloat16)
    expert_in = rms_rows(resid, expert_gain)
    topk = routes.shape[1]
    e_loc = expert_gate.shape[0]
    n_exp = e_loc * n_ep
    cap = max(2, 2 * seqs * topk // n_exp)
    half_width = width // lax.axis_size("tp")
    flat = routes.reshape(-1)
    onehot = (flat[:, None] == jnp.arange(n_exp, dtype=jnp.int32)[None, :]).astype(jnp.int32)
    rank = jnp.sum((jnp.cumsum(onehot, axis=0) - onehot) * onehot, axis=-1)
    slot = flat * cap + rank
    dispatch = (jnp.arange(n_exp * cap, dtype=jnp.int32)[:, None] == slot[None, :]).astype(
        jnp.bfloat16
    )
    repeated = jnp.repeat(expert_in, topk, axis=0)
    send = (
        jnp.dot(dispatch, repeated, preferred_element_type=jnp.float32)
        .astype(jnp.bfloat16)
        .reshape(n_exp, cap, width)
    )
    received = lax.all_to_all(send, "ep", split_axis=0, concat_axis=0, tiled=True)
    slots = received.shape[1]
    grouped = received.reshape(n_ep, e_loc, slots, width)
    partial_exp = expert_ffn(grouped, expert_gate, expert_up, expert_down)
    halves = sent_and_summed(partial_exp.astype(jnp.bfloat16), "tp", 3)
    outputs = halves.astype(jnp.bfloat16).reshape(n_ep * e_loc, slots, half_width)
    returned = lax.all_to_all(outputs, "ep", split_axis=0, concat_axis=0, tiled=True)
    picked = jnp.dot(
        dispatch.T, returned.reshape(n_exp * cap, half_width), preferred_element_type=jnp.float32
    )
    moe = jnp.sum(picked.reshape(seqs, topk, half_width) * route_weights[:, :, None], axis=1)
    resid_half = lax.dynamic_slice_in_dim(
        resid.astype(jnp.float32), lax.axis_index("tp") * half_width, half_width, 1
    )
    return (resid_half + moe).astype(jnp.bfloat16)


def solution(mesh):
    in_specs = (
        P("ep", None),
        P(),
        P(),
        P(None, "tp"),
        P(None, "tp"),
        P(None, "tp"),
        P(),
        P("tp", None),
        P("ep", None, "tp", None),
        P("ep", None, "tp", None),
        P("ep", "tp", None),
        P("ep"),
        P("ep", None),
        P("ep", None),
        P("ep", None, "tp"),
        P("ep", None, "tp"),
        P("ep", "tp", None),
    )
    out_specs = P("ep", "tp")
    return jax.shard_map(shards, mesh=mesh, in_specs=in_specs, out_specs=out_specs, check_vma=False)
```

profile of v0, /device:TPU:1, one launch (start us, length us, event | category | flops | bytes accessed | tf_op | source)
XLA Modules:
  0.0 117.5 jit_solution(3619117313486683096)
XLA Ops:
  0.0 0.0 copy-start
  0.0 0.0 copy-start.1
  0.0 0.0 copy-start.6
  0.0 0.8 broadcast_add_fusion
  0.8 0.8 iota_compare_fusion.3
  1.6 0.7 convert_element_type.87
  2.2 1.1 fusion.35
  3.3 1.7 %fusion.51 = f32[48]{0:T(128)S(1)} fusion(f32[48,1,1024]{2,1,0:T(1,128)} %param.27, s32[48]{0:T(128)S(1)} %broadcast_add_fusion), kind=kLoop, calls=%fused_computation.62 | loop fusion | flops 147408 | bytes 196992 | tf_op jit(solution)/shard_map/reduce_sum | solution.py:49
  5.0 1.2 %fusion.62 = f32[48]{0:T(128)S(1)} fusion(f32[48]{0:T(128)S(1)} %fusion.51, bf16[2048,2]{0,1:T(2,128)(2,1)} %param.23, s32[]{:T(128)S(6)} %select_n.21, bf16[48,2048]{1,0:T(8,128)(2,1)} %param.17, f32[2048]{0:T(1024)S(1)} %convert_element_type.87, f32[48]{0:T(128)S(1)} %add_rsqrt_fusion.1), kind=kOutput, calls=%fused_computation.87 | convolution fusion | flops 590256 | bytes 213572 | tf_op jit(solution)/shard_map/dot_general | solution.py:105
  6.2 1.1 broadcast_subtract_fusion
  7.4 1.7 %convolution_convert_fusion.3 = bf16[48,256]{1,0:T(8,128)(2,1)S(1)} fusion(bf16[2048,256]{1,0:T(8,128)(2,1)} %param.20, bf16[48,2048]{1,0:T(8,128)(2,1)} %param.17, f32[2048]{0:T(1024)S(1)} %convert_element_type.87, f32[48]{0:T(128)S(1)} %add_rsqrt_fusion.1), kind=kOutput, calls=%fused_computation.17 | convolution fusion | flops 50737152 | bytes 1278144 | tf_op jit(solution)/shard_map/dot_general | solution.py:107
  9.1 0.0 copy-done.1
  9.1 0.0 copy-done.6
  9.1 0.3 fusion.17
  9.4 0.2 fusion.56
  9.6 0.0 copy-start.7
  9.6 8.1 %fusion.72 = (f32[48,2]{1,0:T(8,128)S(1)}, f32[48,2,1024]{2,1,0:T(2,128)S(1)}) fusion(f32[48,1024]{1,0:T(8,128)S(1)} %bitcast.107, bf16[48,2,128]{2,1,0:T(2,128)(2,1)S(1)} %reshape.247, bf16[48,1024,1,128]{3,1,2,0:T(8,128)(2,1)} %param.25, pred[48,1024]{1,0:T(8,128)(4,1)S(1)} %iota_compare_fusion.3), kind=kOutput, calls=%fused_computation.93 | convolution fusion | flops 25558944 | bytes 13246848 | tf_op jit(solution)/shard_map/skgd,slkd->skgl/dot_general | solution.py:54
  17.7 0.4 fusion.45
  18.1 0.0 copy-done.7
  18.2 0.3 fusion.16
  18.4 0.0 copy-start.5
  18.4 5.8 %fusion.21 = bf16[48,2,128]{2,1,0:T(2,128)(2,1)S(1)} fusion(bf16[48,1024,1,128]{3,1,2,0:T(8,128)(2,1)} %param.26, f32[48,2,1024]{2,1,0:T(2,128)S(1)} %get-tuple-element.10, f32[48,2]{1,0:T(8,128)S(1)} %get-tuple-element.8, f32[48,2]{1,0:T(8,128)S(1)} %multiply_maximum_fusion, f32[48,128]{1,0:T(8,128)S(1)} %fusion.16, f32[48,2]{1,0:T(8,128)S(1)} %get-tuple-element.7), kind=kOutput, calls=%fused_computation.25 | convolution fusion | flops 25497600 | bytes 13026432 | tf_op jit(solution)/shard_map/skgl,slkd->skgd/dot_general | solution.py:66
  24.2 0.0 copy-done.5
  24.2 0.0 copy-start.8
  24.3 0.3 convolution_convert_fusion.2
  24.6 5.0 %all_to_all.20 = bf16[2,48,2048]{2,1,0:T(8,128)(2,1)S(1)} all-to-all(bf16[2,48,2048]{2,1,0:T(8,128)(2,1)S(1)} %broadcast_in_dim.23), channel_id=1, replica_groups=mesh['ep'=64,'tp'=2] {'tp'}, dimensions={0} | all-to-all | bytes 786432 | tf_op jit(solution)/shard_map/all_to_all | solution.py:11
  29.6 0.1 convert_reduce_fusion
  29.7 0.0 copy-start.9
  29.7 0.2 multiply_reduce_fusion
  29.9 0.0 copy-start.2
  29.9 0.0 copy-done.8
  29.9 0.7 copy-done.2
  30.7 0.1 multiply_convert_fusion
  30.8 0.4 broadcast_in_dim.24
  31.1 0.2 reshape.255
  31.3 0.0 copy-done.9
  31.3 0.1 copy.42
  31.4 0.1 reshape.252
  31.6 0.6 reduce-window.6
  32.2 0.2 slice_reduce_fusion
  32.4 0.1 bitcast_bitcast_fusion.1
  32.6 1.7 %convolution_convert_fusion.1 = bf16[384,2048]{1,0:T(8,128)(2,1)} fusion(bf16[192,2048]{1,0:T(8,128)(2,1)S(1)} %reshape.255, s32[192]{0:T(256)S(1)} %multiply_add_fusion), kind=kOutput, calls=%fused_computation.5 | convolution fusion | flops 302850048 | bytes 2360064 | tf_op jit(solution)/shard_map/dot_general | solution.py:133
  34.3 2.5 %reshape.256 = bf16[64,6,2048]{2,1,0:T(8,128)(2,1)S(1)} reshape(bf16[384,2048]{1,0:T(8,128)(2,1)} %convolution_convert_fusion.1) | data formatting | bytes 3145728 | tf_op jit(solution)/shard_map/reshape | solution.py:135
  36.8 0.0 copy-start.10
  36.8 40.2 %all_to_all.21 = bf16[64,6,2048]{2,1,0:T(8,128)(2,1)S(1)} all-to-all(bf16[64,6,2048]{2,1,0:T(8,128)(2,1)S(1)} %reshape.256), channel_id=1, replica_groups=mesh['ep'=64,'tp'=2] {'ep'}, dimensions={0} | all-to-all | bytes 3145728 | tf_op jit(solution)/shard_map/all_to_all | solution.py:137
  76.9 0.0 copy-start.4
  76.9 1.3 %copy-done.4 = bf16[64,6,2048]{2,1,0:T(8,128)(2,1)} copy-done((bf16[64,6,2048]{2,1,0:T(8,128)(2,1)}, bf16[64,6,2048]{2,1,0:T(8,128)(2,1)S(1)}, u32[]{:S(2)}) %copy-start.4) | copy-done | bytes 1572888
  78.3 0.0 copy-done.10
  78.3 1.8 %convolution_bitcast_fusion.1 = f32[64,1,6,256]{3,0,2,1:T(8,128)S(1)} fusion(bf16[64,6,2048]{2,1,0:T(8,128)(2,1)S(1)} %all_to_all.21, bf16[1,2048,256]{2,1,0:T(8,128)(2,1)S(1)} %copy-done.10), kind=kOutput, calls=%fused_computation.12 | convolution fusion | flops 402653184 | bytes 3014656 | tf_op jit(solution)/shard_map/necd,edf->necf/dot_general | solution.py:74
  80.1 0.0 copy-done
  80.1 3.7 %convolution_convert_fusion = bf16[64,6,2048]{2,0,1:T(8,128)(2,1)S(1)} fusion(bf16[1,256,2048]{2,1,0:T(8,128)(2,1)S(1)} %copy-done, bf16[64,6,2048]{2,1,0:T(8,128)(2,1)} %copy-done.4, bf16[1,2048,256]{2,1,0:T(8,128)(2,1)} %param.32, f32[64,1,6,256]{3,0,2,1:T(8,128)S(1)} %convolution_bitcast_fusion.1), kind=kOutput, calls=%fused_computation.4 | convolution fusion | flops 806682624 | bytes 5636096 | tf_op jit(solution)/shard_map/necf,efd->necd/dot_general | solution.py:77
  83.8 0.1 copy.77
  83.9 6.7 %all_to_all.22 = bf16[2,64,1,6,1024]{4,1,3,2,0:T(8,128)(2,1)S(1)} all-to-all(bf16[2,64,1,6,1024]{4,1,3,2,0:T(8,128)(2,1)S(1)} %bitcast.105), channel_id=1, replica_groups=mesh['ep'=64,'tp'=2] {'tp'}, dimensions={0} | all-to-all | bytes 3145728 | tf_op jit(solution)/shard_map/all_to_all | solution.py:27
  90.6 0.4 reduce_sum.81
  91.0 1.4 %copy.49 = bf16[64,6,1024]{2,1,0:T(8,128)(2,1)} copy(bf16[64,6,1024]{2,0,1:T(8,128)(2,1)S(1)} %reduce_sum.81) | data formatting | bytes 1572864 | tf_op jit(solution)/shard_map/reduce_sum | solution.py:28
  92.5 5.6 %all-to-all-start.3 = ((bf16[64,6,1024]{2,1,0:T(8,128)(2,1)}), bf16[64,6,1024]{2,1,0:T(8,128)(2,1)S(1)}, u32[]{:S(2)}, u32[]{:S(2)}) async-start(bf16[64,6,1024]{2,1,0:T(8,128)(2,1)} %copy.49), calls=%async_computation.3 | async-start | bytes 2097152 | tf_op jit(solution)/shard_map/all_to_all | solution.py:143
  98.0 0.0 copy-start.3
  98.0 0.1 iota_compare_fusion.2
  98.2 17.9 %all-to-all-done.3 = bf16[64,6,1024]{2,1,0:T(8,128)(2,1)S(1)} async-done(((bf16[64,6,1024]{2,1,0:T(8,128)(2,1)}), bf16[64,6,1024]{2,1,0:T(8,128)(2,1)S(1)}, u32[]{:S(2)}, u32[]{:S(2)}) %all-to-all-start.3) | async-done | bytes 786464 | tf_op jit(solution)/shard_map/all_to_all | solution.py:143
  116.1 0.3 reshape.271
  116.4 0.0 copy-done.11
  116.4 0.4 fusion.4
  116.8 0.0 copy-done.3
  116.8 0.7 add_convert_fusion
  (16 shorter events, 0.3 us)
Async XLA Ops:
  0.0 80.1 %copy-start = (bf16[1,256,2048]{2,1,0:T(8,128)(2,1)S(1)}, bf16[1,256,2048]{2,1,0:T(8,128)(2,1)}, u32[]{:S(2)}) copy-start(bf16[1,256,2048]{2,1,0:T(8,128)(2,1)} %param.33) | copy-start | bytes 3145732
  0.0 9.1 %copy-start.1 = (bf16[48,2048]{1,0:T(8,128)(2,1)S(1)}, bf16[48,2048]{1,0:T(8,128)(2,1)}, u32[]{:S(2)}) copy-start(bf16[48,2048]{1,0:T(8,128)(2,1)} %param.17) | copy-start | bytes 589828
  0.0 9.1 %copy-start.6 = (bf16[2048,128]{1,0:T(8,128)(2,1)S(1)}, bf16[2048,128]{1,0:T(8,128)(2,1)}, u32[]{:S(2)}) copy-start(bf16[2048,128]{1,0:T(8,128)(2,1)} %param.21) | copy-start | bytes 1572868
  9.6 8.6 %copy-start.7 = (bf16[2048,128]{1,0:T(8,128)(2,1)S(1)}, bf16[2048,128]{1,0:T(8,128)(2,1)}, u32[]{:S(2)}) copy-start(bf16[2048,128]{1,0:T(8,128)(2,1)} %param.22) | copy-start | bytes 1572868
  18.4 5.8 %copy-start.5 = (bf16[256,2048]{1,0:T(8,128)(2,1)S(1)}, bf16[256,2048]{1,0:T(8,128)(2,1)}, u32[]{:S(2)}) copy-start(bf16[256,2048]{1,0:T(8,128)(2,1)} %param.24) | copy-start | bytes 3145732
  24.2 5.7 %copy-start.8 = (bf16[2048]{0:T(1024)(128)(2,1)S(1)}, bf16[2048]{0:T(1024)(128)(2,1)}, u32[]{:S(2)}) copy-start(bf16[2048]{0:T(1024)(128)(2,1)} %param.19) | copy-start | bytes 12292
  29.7 1.6 %copy-start.9 = (s32[48,4]{0,1:T(4,128)S(1)}, s32[48,4]{0,1:T(4,128)}, u32[]{:S(2)}) copy-start(s32[48,4]{0,1:T(4,128)} %param.29) | copy-start | bytes 2308
  29.9 0.8 copy-start.2
  36.8 41.5 %copy-start.10 = (bf16[1,2048,256]{2,1,0:T(8,128)(2,1)S(1)}, bf16[1,2048,256]{2,1,0:T(8,128)(2,1)}, u32[]{:S(2)}) copy-start(bf16[1,2048,256]{2,1,0:T(8,128)(2,1)} %param.31) | copy-start | bytes 3145732
  76.9 1.4 %copy-start.4 = (bf16[64,6,2048]{2,1,0:T(8,128)(2,1)}, bf16[64,6,2048]{2,1,0:T(8,128)(2,1)S(1)}, u32[]{:S(2)}) copy-start(bf16[64,6,2048]{2,1,0:T(8,128)(2,1)S(1)} %all_to_all.21) | copy-start | bytes 4718596
  92.5 23.9 %copy-start.11 = (f32[48,4]{0,1:T(4,128)S(1)}, f32[48,4]{0,1:T(4,128)}, u32[]{:S(2)}) copy-start(f32[48,4]{0,1:T(4,128)} %param.30) | copy-start | bytes 2308
  92.5 23.6 %all-to-all-start.3 = ((bf16[64,6,1024]{2,1,0:T(8,128)(2,1)}), bf16[64,6,1024]{2,1,0:T(8,128)(2,1)S(1)}, u32[]{:S(2)}, u32[]{:S(2)}) async-start(bf16[64,6,1024]{2,1,0:T(8,128)(2,1)} %copy.49), calls=%async_computation.3 | async-start | bytes 2097152 | tf_op jit(solution)/shard_map/all_to_all | solution.py:143
  98.0 18.7 %copy-start.3 = (f32[48,2048]{1,0:T(8,128)S(1)}, f32[48,2048]{1,0:T(8,128)}, u32[]{:S(2)}) copy-start(f32[48,2048]{1,0:T(8,128)} %copy-done.2) | copy-start | bytes 1179652
where the time goes:
time: 118 us; the launch traced here: 117 us
  blocking collectives  51.9 us (44%)
  matrix products  25.3 us (21%)
  waiting for transfers between devices  17.9 us (15%)
  other arithmetic  8.9 us (8%)
  local copies, waits for them, and re-layouts  7.49 us (6%)
  starting transfers between devices  5.55 us (5%)
    all_to_all x1, blocking collectives, shards(): lax.all_to_all(send, 'ep', split_axis=0, concat_axis=0, tiled=True)  40.2 us
    all_to_all x1, waiting for transfers between devices, shards(): lax.all_to_all(outputs, 'ep', split_axis=0, concat_axis=0, tiled=True)  17.9 us
    dot_general x1, matrix products, attend(): jnp.einsum('skgd,slkd->skgl', q_four, key_cache, preferred_element_type=j...  8.11 us
    all_to_all x1, blocking collectives, sent_and_summed(): lax.all_to_all(blocks, axis, split_axis=0, concat_axis=0, tiled=True)  6.69 us
    dot_general x1, matrix products, attend(): jnp.einsum('skgl,slkd->skgd', probs, cached_values, preferred_element_typ...  5.78 us
    all_to_all x1, starting transfers between devices, shards(): lax.all_to_all(outputs, 'ep', split_axis=0, concat_axis=0, tiled=True)  5.55 us
    all_to_all x1, blocking collectives, sent_to_all(): lax.all_to_all(jnp.broadcast_to(array[None], (size, *array.shape)), axis,...  5.05 us
    dot_general x1, matrix products, expert_ffn(): jnp.einsum('necf,efd->necd', act, down_w, preferred_element_type=jnp.floa...  3.7 us
  transfers between devices with their start and end apart: 1, of which 1 were waited for; matrix products, arithmetic and copies ran while one was open for 0% of the time, Pallas kernels for 0%

commit v1 on v0

--- a/solution.py
+++ b/solution.py
@@ -4,28 +4,6 @@
 from jax.sharding import PartitionSpec as P
 
 EPS = 1e-06
-
-
-def sent_to_all(array, axis):
-    size = lax.axis_size(axis)
-    return lax.all_to_all(
-        jnp.broadcast_to(array[None], (size, *array.shape)), axis, 0, 0, tiled=True
-    )
-
-
-def of_everyone(array, axis):
-    return sent_to_all(array, axis).astype(jnp.float32).sum(axis=0)
-
-
-def cut_along(array, dim, size):
-    before, after = (array.shape[:dim], array.shape[dim + 1 :])
-    return jnp.moveaxis(array.reshape(*before, size, -1, *after), dim, 0)
-
-
-def sent_and_summed(array, axis, dim):
-    blocks = cut_along(array, dim, lax.axis_size(axis))
-    arrived = lax.all_to_all(blocks, axis, split_axis=0, concat_axis=0, tiled=True)
-    return arrived.astype(jnp.float32).sum(axis=0)
 
 
 def rms_rows(values, gain):
@@ -70,13 +48,6 @@
     return result.astype(jnp.bfloat16).reshape(seqs, kv_heads * group * head_size)
 
 
-def expert_ffn(received, gate_w, up_w, down_w):
-    gate = jnp.einsum("necd,edf->necf", received, gate_w, preferred_element_type=jnp.float32)
-    upper = jnp.einsum("necd,edf->necf", received, up_w, preferred_element_type=jnp.float32)
-    act = (jax.nn.silu(gate) * upper).astype(jnp.bfloat16)
-    return jnp.einsum("necf,efd->necd", act, down_w, preferred_element_type=jnp.float32)
-
-
 def shards(
     tokens,
     norm_gain,
@@ -112,43 +83,55 @@
     attended = attend(
         query_rows, key_new, value_new, log_forget, key_cache, cached_values, cum_gates, lengths
     )
-    partial_out = jnp.dot(attended, w_out, preferred_element_type=jnp.float32)
-    mixed = of_everyone(partial_out.astype(jnp.bfloat16), "tp").astype(jnp.float32)
+    swap = [(0, 1), (1, 0)]
+    core = lax.axis_index("tp")
+    partial_out = jnp.dot(attended, w_out, preferred_element_type=jnp.float32).astype(jnp.bfloat16)
+    other_out = lax.ppermute(partial_out, "tp", swap)
+    mixed = partial_out.astype(jnp.float32) + other_out.astype(jnp.float32)
     resid = (tokens.astype(jnp.float32) + mixed).astype(jnp.bfloat16)
     expert_in = rms_rows(resid, expert_gain)
     topk = routes.shape[1]
-    e_loc = expert_gate.shape[0]
-    n_exp = e_loc * n_ep
+    n_exp = expert_gate.shape[0] * n_ep
     cap = max(2, 2 * seqs * topk // n_exp)
-    half_width = width // lax.axis_size("tp")
+    share = cap // 2
+    gate_own, up_own, down_own = expert_gate[0], expert_up[0], expert_down[0]
+    gate_peer, up_peer, down_peer = (
+        lax.ppermute(w, "tp", swap) for w in (gate_own, up_own, down_own)
+    )
     flat = routes.reshape(-1)
-    onehot = (flat[:, None] == jnp.arange(n_exp, dtype=jnp.int32)[None, :]).astype(jnp.int32)
-    rank = jnp.sum((jnp.cumsum(onehot, axis=0) - onehot) * onehot, axis=-1)
-    slot = flat * cap + rank
-    dispatch = (jnp.arange(n_exp * cap, dtype=jnp.int32)[:, None] == slot[None, :]).astype(
+    order = jnp.arange(flat.shape[0], dtype=jnp.int32)
+    earlier = (flat[:, None] == flat[None, :]) & (order[None, :] < order[:, None])
+    rank = jnp.sum(earlier.astype(jnp.int32), axis=-1) - core * share
+    slot = jnp.where((rank >= 0) & (rank < share), flat * share + rank, -1)
+    dispatch = (jnp.arange(n_exp * share, dtype=jnp.int32)[:, None] == slot[None, :]).astype(
         jnp.bfloat16
     )
     repeated = jnp.repeat(expert_in, topk, axis=0)
-    send = (
-        jnp.dot(dispatch, repeated, preferred_element_type=jnp.float32)
-        .astype(jnp.bfloat16)
-        .reshape(n_exp, cap, width)
-    )
+    send = jnp.dot(dispatch, repeated, preferred_element_type=jnp.float32).astype(jnp.bfloat16)
+    send = send.reshape(n_exp, share * width // 128, 128)
     received = lax.all_to_all(send, "ep", split_axis=0, concat_axis=0, tiled=True)
-    slots = received.shape[1]
-    grouped = received.reshape(n_ep, e_loc, slots, width)
-    partial_exp = expert_ffn(grouped, expert_gate, expert_up, expert_down)
-    halves = sent_and_summed(partial_exp.astype(jnp.bfloat16), "tp", 3)
-    outputs = halves.astype(jnp.bfloat16).reshape(n_ep * e_loc, slots, half_width)
+    rows = received.reshape(n_exp * share, width)
+
+    def hidden(gate_w, up_w):
+        gate = jnp.dot(rows, gate_w, preferred_element_type=jnp.float32)
+        upper = jnp.dot(rows, up_w, preferred_element_type=jnp.float32)
+        return (jax.nn.silu(gate) * upper).astype(jnp.bfloat16)
+
+    outputs = jnp.dot(
+        hidden(gate_own, up_own), down_own, preferred_element_type=jnp.float32
+    ) + jnp.dot(hidden(gate_peer, up_peer), down_peer, preferred_element_type=jnp.float32)
+    outputs = outputs.astype(jnp.bfloat16).reshape(n_exp, share * width // 128, 128)
     returned = lax.all_to_all(outputs, "ep", split_axis=0, concat_axis=0, tiled=True)
     picked = jnp.dot(
-        dispatch.T, returned.reshape(n_exp * cap, half_width), preferred_element_type=jnp.float32
+        dispatch.T, returned.reshape(n_exp * share, width), preferred_element_type=jnp.float32
     )
-    moe = jnp.sum(picked.reshape(seqs, topk, half_width) * route_weights[:, :, None], axis=1)
-    resid_half = lax.dynamic_slice_in_dim(
-        resid.astype(jnp.float32), lax.axis_index("tp") * half_width, half_width, 1
-    )
-    return (resid_half + moe).astype(jnp.bfloat16)
+    moe = jnp.sum(picked.reshape(seqs, topk, width) * route_weights[:, :, None], axis=1)
+    half = width // 2
+    keep = lax.dynamic_slice_in_dim(moe, core * half, half, 1)
+    give = lax.dynamic_slice_in_dim(moe, (1 - core) * half, half, 1)
+    got = lax.ppermute(give, "tp", swap)
+    resid_half = lax.dynamic_slice_in_dim(resid.astype(jnp.float32), core * half, half, 1)
+    return (resid_half + (keep + got)).astype(jnp.bfloat16)
 
 
 def solution(mesh):

time: 118 us -> 93.8 us (0.79)
  blocking collectives: 51.9 us -> 0 us
  starting transfers between devices: 5.55 us -> 21.8 us
  waiting for transfers between devices: 17.9 us -> 29.6 us
  matrix products: 25.3 us -> 27.9 us
  local copies, waits for them, and re-layouts: 7.49 us -> 5.7 us
    all_to_all x3 -> x0, blocking collectives: 51.9 us -> none  [the longest x1 40.2 us: shards(): lax.all_to_all(send, 'ep', split_axis=0, concat_axis=0, tiled=True)]
    all_to_all x0 -> x1, waiting for transfers between devices: none -> 14 us  [shards(): lax.all_to_all(send, 'ep', split_axis=0, concat_axis=0, tiled=True)]
    all_to_all x0 -> x1, starting transfers between devices: none -> 11.3 us  [shards(): lax.all_to_all(send, 'ep', split_axis=0, concat_axis=0, tiled=True)]
    ppermute x0 -> x5, starting transfers between devices: none -> 5.79 us  [the longest x1 3.1 us: shards(): got = lax.ppermute(give, 'tp', swap)]
    dot_general x4 -> x6, matrix products: 6.16 us -> 11.5 us  [the longest x2 4.57 us: hidden(): gate = jnp.dot(rows, gate_w, preferred_element_type=jnp.float32)]
    all_to_all x1, waiting for transfers between devices: 17.9 us -> 13.9 us  [shards(): lax.all_to_all(outputs, 'ep', split_axis=0, concat_axis=0, tiled=True)]
    ppermute x0 -> x5, waiting for transfers between devices: none -> 1.74 us  [the longest x1 1.07 us: shards(): got = lax.ppermute(give, 'tp', swap)]
    reduce_sum x1 -> x0, local copies, waits for them, and re-layouts: 1.43 us -> none  [sent_and_summed(): return arrived.astype(jnp.float32).sum(axis=0)]
  transfers between devices with their start and end apart: 1 -> 7, of which waited for: 1 -> 4; matrix products, arithmetic and copies ran while one was open for 0% -> 9% of each run, Pallas kernels for 0% -> 0%
where the time goes in v1:
time: 93.8 us; the launch traced here: 93.2 us
  waiting for transfers between devices  29.6 us (32%)
  matrix products  27.9 us (30%)
  starting transfers between devices  21.8 us (23%)
  other arithmetic  7.91 us (8%)
  local copies, waits for them, and re-layouts  5.7 us (6%)
    all_to_all x1, waiting for transfers between devices, shards(): lax.all_to_all(send, 'ep', split_axis=0, concat_axis=0, tiled=True)  14 us
    all_to_all x1, waiting for transfers between devices, shards(): lax.all_to_all(outputs, 'ep', split_axis=0, concat_axis=0, tiled=True)  13.9 us
    all_to_all x1, starting transfers between devices, shards(): lax.all_to_all(send, 'ep', split_axis=0, concat_axis=0, tiled=True)  11.3 us
    dot_general x1, matrix products, attend(): jnp.einsum('skgd,slkd->skgl', q_four, key_cache, preferred_element_type=j...  8.07 us
    dot_general x1, matrix products, attend(): jnp.einsum('skgl,slkd->skgd', probs, cached_values, preferred_element_typ...  5.71 us
    all_to_all x1, starting transfers between devices, shards(): lax.all_to_all(outputs, 'ep', split_axis=0, concat_axis=0, tiled=True)  4.77 us
    dot_general x2, matrix products, hidden(): gate = jnp.dot(rows, gate_w, preferred_element_type=jnp.float32)  4.57 us
    dot_general x1, matrix products, shards(): jnp.dot(hidden(gate_peer, up_peer), down_peer, preferred_element_type=jnp...  3.6 us
  transfers between devices with their start and end apart: 7, of which 4 were waited for; matrix products, arithmetic and copies ran while one was open for 9% of the time, Pallas kernels for 0%

profile of v1, /device:TPU:1, one launch (start us, length us, event | category | flops | bytes accessed | tf_op | source)
XLA Modules:
  0.0 93.2 jit_solution(1633195016204290350)
XLA Ops:
  0.0 0.0 copy-start
  0.0 0.0 copy-start.5
  0.0 0.8 broadcast_add_fusion
  0.8 0.8 iota_compare_fusion.3
  1.6 0.7 convert_element_type.81
  2.3 1.1 %fusion.26 = f32[48]{0:T(128)S(1)} fusion(bf16[48,2048]{1,0:T(8,128)(2,1)} %param.17), kind=kLoop, calls=%fused_computation.29 | loop fusion | flops 294864 | bytes 196800 | tf_op jit(solution)/shard_map/reduce_sum | solution.py:11
  3.4 1.7 %fusion.39 = f32[48]{0:T(128)S(1)} fusion(f32[48,1,1024]{2,1,0:T(1,128)} %param.27, s32[48]{0:T(128)S(1)} %broadcast_add_fusion), kind=kLoop, calls=%fused_computation.54 | loop fusion | flops 147408 | bytes 196992 | tf_op jit(solution)/shard_map/reduce_sum | solution.py:27
  5.1 1.2 %fusion.54 = f32[48]{0:T(128)S(1)} fusion(f32[48]{0:T(128)S(1)} %fusion.39, bf16[2048,2]{0,1:T(2,128)(2,1)} %param.23, s32[]{:T(128)S(6)} %select_n.33, bf16[48,2048]{1,0:T(8,128)(2,1)} %param.17, f32[2048]{0:T(1024)S(1)} %convert_element_type.81, f32[48]{0:T(128)S(1)} %add_rsqrt_fusion.1), kind=kOutput, calls=%fused_computation.76 | convolution fusion | flops 590256 | bytes 213572 | tf_op jit(solution)/shard_map/dot_general | solution.py:76
  6.3 1.1 %broadcast_subtract_fusion = f32[48,1,1024]{2,1,0:T(1,128)S(1)} fusion(f32[48,1,1024]{2,1,0:T(1,128)} %param.27, f32[48]{0:T(128)S(1)} %fusion.54), kind=kLoop, calls=%fused_computation.57 | loop fusion | flops 49152 | bytes 393408 | tf_op jit(solution)/shard_map/sub | solution.py:30
  7.5 0.0 copy-done.1
  7.5 0.0 copy-done.4
  7.5 0.3 convolution_convert_fusion.2
  7.8 0.0 copy-done.5
  7.9 0.3 fusion.15
  8.1 0.2 fusion.47
  8.3 0.0 copy-start.6
  8.3 8.1 %fusion.69 = (f32[48,2]{1,0:T(8,128)S(1)}, f32[48,2,1024]{2,1,0:T(2,128)S(1)}) fusion(f32[48,1024]{1,0:T(8,128)S(1)} %bitcast.63, bf16[48,2,128]{2,1,0:T(2,128)(2,1)S(1)} %reshape.218, bf16[48,1024,1,128]{3,1,2,0:T(8,128)(2,1)} %param.25, pred[48,1024]{1,0:T(8,128)(4,1)S(1)} %iota_compare_fusion.3), kind=kOutput, calls=%fused_computation.86 | convolution fusion | flops 25558944 | bytes 13246848 | tf_op jit(solution)/shard_map/skgd,slkd->skgl/dot_general | solution.py:32
  16.4 0.4 fusion.30
  16.9 0.0 copy-done.6
  16.9 0.3 fusion.14
  17.1 0.0 copy-start.7
  17.2 0.0 copy-start.8
  17.2 5.7 %fusion.19 = bf16[48,2,128]{2,1,0:T(2,128)(2,1)S(1)} fusion(bf16[48,1024,1,128]{3,1,2,0:T(8,128)(2,1)} %param.26, f32[48,2,1024]{2,1,0:T(2,128)S(1)} %get-tuple-element.10, f32[48,2]{1,0:T(8,128)S(1)} %get-tuple-element.8, f32[48,2]{1,0:T(8,128)S(1)} %multiply_maximum_fusion, f32[48,128]{1,0:T(8,128)S(1)} %fusion.14, f32[48,2]{1,0:T(8,128)S(1)} %get-tuple-element.7), kind=kOutput, calls=%fused_computation.21 | convolution fusion | flops 25497600 | bytes 13026432 | tf_op jit(solution)/shard_map/skgl,slkd->skgd/dot_general | solution.py:44
  22.9 0.0 copy-done
  22.9 0.3 convolution_convert_fusion.1
  23.2 1.5 %collective-permute-start = (bf16[48,2048]{1,0:T(8,128)(2,1)S(1)}, bf16[48,2048]{1,0:T(8,128)(2,1)S(1)}, u32[]{:S(2)}, u32[]{:S(2)}) collective-permute-start(bf16[48,2048]{1,0:T(8,128)(2,1)S(1)} %convolution_convert_fusion.1), channel_id=1, source_target_pairs={{0,1},{1,0},{2,3},{3,2},{4,5},{5,4},{6,7},{7,6},{8,9},{9,8},{10,11... | collective-permute-start | bytes 589832 | tf_op jit(solution)/shard_map/ppermute | solution.py:89
  24.7 0.0 copy-done.7
  24.7 0.0 copy-done.8
  24.7 0.1 copy.20
  24.8 0.1 eq.70
  24.9 0.2 convert_reduce_fusion
  25.1 0.7 collective-permute-done
  25.7 0.2 multiply_reduce_fusion
  25.9 0.7 copy-done.2
  26.7 0.1 multiply_convert_fusion
  26.8 0.4 broadcast_in_dim.25
  27.1 0.2 reshape.223
  27.3 0.4 convolution_convert_fusion
  27.7 1.2 %reshape.224 = bf16[64,48,128]{2,1,0:T(8,128)(2,1)} reshape(bf16[192,2048]{1,0:T(8,128)(2,1)S(1)} %convolution_convert_fusion) | data formatting | bytes 1572864 | tf_op jit(solution)/shard_map/reshape | solution.py:111
  28.9 11.3 %all-to-all-start = ((bf16[64,48,128]{2,1,0:T(8,128)(2,1)}), bf16[64,48,128]{2,1,0:T(8,128)(2,1)S(1)}, u32[]{:S(2)}, u32[]{:S(2)}) async-start(bf16[64,48,128]{2,1,0:T(8,128)(2,1)} %reshape.224), calls=%async_computation | async-start | bytes 1572864 | tf_op jit(solution)/shard_map/all_to_all | solution.py:112
  40.2 0.7 collective-permute-start.1
  40.9 0.1 collective-permute-start.2
  41.0 0.4 collective-permute-start.3
  41.4 14.0 %all-to-all-done = bf16[64,48,128]{2,1,0:T(8,128)(2,1)S(1)} async-done(((bf16[64,48,128]{2,1,0:T(8,128)(2,1)}), bf16[64,48,128]{2,1,0:T(8,128)(2,1)S(1)}, u32[]{:S(2)}, u32[]{:S(2)}) %all-to-all-start) | async-done | bytes 786464 | tf_op jit(solution)/shard_map/all_to_all | solution.py:112
  55.4 0.3 reshape.225
  55.7 2.3 %fusion.60 = f32[192,256]{1,0:T(8,128)} fusion(bf16[192,2048]{1,0:T(8,128)(2,1)S(1)} %reshape.225, bf16[1,2048,256]{2,1,0:T(8,128)(2,1)} %param.31), kind=kOutput, calls=%fused_computation.82 | convolution fusion | flops 201326592 | bytes 2031616 | tf_op jit(solution)/shard_map/dot_general | solution.py:116
  58.0 2.7 %fusion.7 = f32[192,2048]{1,0:T(8,128)S(1)} fusion(bf16[192,2048]{1,0:T(8,128)(2,1)S(1)} %reshape.225, f32[192,256]{1,0:T(8,128)} %fusion.60, bf16[1,256,2048]{2,1,0:T(8,128)(2,1)} %param.33, bf16[1,2048,256]{2,1,0:T(8,128)(2,1)} %param.32), kind=kOutput, calls=%fused_computation.12 | convolution fusion | flops 402948096 | bytes 4653056 | tf_op jit(solution)/shard_map/dot_general | solution.py:120
  60.7 0.0 collective-permute-done.1
  60.7 2.3 %fusion.72 = f32[192,256]{1,0:T(8,128)} fusion(bf16[192,2048]{1,0:T(8,128)(2,1)S(1)} %reshape.225, bf16[2048,256]{1,0:T(8,128)(2,1)} %collective-permute-done.1), kind=kOutput, calls=%fused_computation.88 | convolution fusion | flops 201326592 | bytes 2031616 | tf_op jit(solution)/shard_map/dot_general | solution.py:116
  63.0 0.0 collective-permute-done.2
  63.0 0.0 collective-permute-done.3
  63.0 3.6 %fusion.4 = bf16[192,2048]{1,0:T(8,128)(2,1)} fusion(f32[192,2048]{1,0:T(8,128)S(1)} %fusion.7, bf16[256,2048]{1,0:T(8,128)(2,1)} %collective-permute-done.3, f32[192,256]{1,0:T(8,128)} %fusion.72, bf16[192,2048]{1,0:T(8,128)(2,1)S(1)} %reshape.225, bf16[2048,256]{1,0:T(8,128)(2,1)} %collective-permute-done.2), kind=kOutput, calls=%fused_computation.6 | convolution fusion | flops 403734528 | bytes 5439488 | tf_op jit(solution)/shard_map/dot_general | solution.py:122
  66.6 2.2 %reshape.226 = bf16[64,48,128]{2,1,0:T(8,128)(2,1)} reshape(bf16[192,2048]{1,0:T(8,128)(2,1)} %fusion.4) | data formatting | bytes 1572864 | tf_op jit(solution)/shard_map/reshape | solution.py:123
  68.8 4.8 %all-to-all-start.1 = ((bf16[64,48,128]{2,1,0:T(8,128)(2,1)}), bf16[64,48,128]{2,1,0:T(8,128)(2,1)S(1)}, u32[]{:S(2)}, u32[]{:S(2)}) async-start(bf16[64,48,128]{2,1,0:T(8,128)(2,1)} %reshape.226), calls=%async_computation.1 | async-start | bytes 1572864 | tf_op jit(solution)/shard_map/all_to_all | solution.py:124
  73.6 0.1 iota_compare_fusion.2
  73.7 0.0 copy-start.3
  73.7 13.9 %all-to-all-done.1 = bf16[64,48,128]{2,1,0:T(8,128)(2,1)S(1)} async-done(((bf16[64,48,128]{2,1,0:T(8,128)(2,1)}), bf16[64,48,128]{2,1,0:T(8,128)(2,1)S(1)}, u32[]{:S(2)}, u32[]{:S(2)}) %all-to-all-start.1) | async-done | bytes 786464 | tf_op jit(solution)/shard_map/all_to_all | solution.py:124
  87.6 0.3 reshape.232
  88.0 0.0 copy-done.9
  88.0 0.4 fusion.5
  88.4 3.1 %collective-permute-start.4 = (f32[48,1024]{1,0:T(8,128)S(1)}, f32[48,1024]{1,0:T(8,128)S(1)}, u32[]{:S(2)}, u32[]{:S(2)}) collective-permute-start(f32[48,1024]{1,0:T(8,128)S(1)} %constant_dynamic-slice_fusion), channel_id=1, source_target_pairs={{0,1},{1,0},{2,3},{3,2},{4,5},{5,4},{6,7},{7,6},{8,9},{9,8},{10,11... | collective-permute-start | bytes 589832 | tf_op jit(solution)/shard_map/ppermute | solution.py:132
  91.5 1.1 %collective-permute-done.4 = f32[48,1024]{1,0:T(8,128)S(1)} collective-permute-done((f32[48,1024]{1,0:T(8,128)S(1)}, f32[48,1024]{1,0:T(8,128)S(1)}, u32[]{:S(2)}, u32[]{:S(2)}) %collective-permute-start.4) | collective-permute-done | bytes 196640 | tf_op jit(solution)/shard_map/ppermute | solution.py:132
  92.6 0.0 copy-done.3
  92.6 0.7 add_convert_fusion
  (14 shorter events, 0.2 us)
Async XLA Ops:
  0.0 22.9 %copy-start = (bf16[256,2048]{1,0:T(8,128)(2,1)S(1)}, bf16[256,2048]{1,0:T(8,128)(2,1)}, u32[]{:S(2)}) copy-start(bf16[256,2048]{1,0:T(8,128)(2,1)} %param.24) | copy-start | bytes 3145732
  0.0 7.5 %copy-start.1 = (bf16[48,2048]{1,0:T(8,128)(2,1)S(1)}, bf16[48,2048]{1,0:T(8,128)(2,1)}, u32[]{:S(2)}) copy-start(bf16[48,2048]{1,0:T(8,128)(2,1)} %param.17) | copy-start | bytes 589828
  0.0 7.5 %copy-start.4 = (bf16[2048,256]{1,0:T(8,128)(2,1)S(1)}, bf16[2048,256]{1,0:T(8,128)(2,1)}, u32[]{:S(2)}) copy-start(bf16[2048,256]{1,0:T(8,128)(2,1)} %param.20) | copy-start | bytes 3145732
  0.0 7.8 %copy-start.5 = (bf16[2048,128]{1,0:T(8,128)(2,1)S(1)}, bf16[2048,128]{1,0:T(8,128)(2,1)}, u32[]{:S(2)}) copy-start(bf16[2048,128]{1,0:T(8,128)(2,1)} %param.21) | copy-start | bytes 1572868
  8.3 8.6 %copy-start.6 = (bf16[2048,128]{1,0:T(8,128)(2,1)S(1)}, bf16[2048,128]{1,0:T(8,128)(2,1)}, u32[]{:S(2)}) copy-start(bf16[2048,128]{1,0:T(8,128)(2,1)} %param.22) | copy-start | bytes 1572868
  17.1 7.5 %copy-start.7 = (bf16[2048]{0:T(1024)(128)(2,1)S(1)}, bf16[2048]{0:T(1024)(128)(2,1)}, u32[]{:S(2)}) copy-start(bf16[2048]{0:T(1024)(128)(2,1)} %param.19) | copy-start | bytes 12292
  17.2 7.5 %copy-start.8 = (s32[48,4]{0,1:T(4,128)S(1)}, s32[48,4]{0,1:T(4,128)}, u32[]{:S(2)}) copy-start(s32[48,4]{0,1:T(4,128)} %param.29) | copy-start | bytes 2308
  23.2 2.5 %collective-permute-start = (bf16[48,2048]{1,0:T(8,128)(2,1)S(1)}, bf16[48,2048]{1,0:T(8,128)(2,1)S(1)}, u32[]{:S(2)}, u32[]{:S(2)}) collective-permute-start(bf16[48,2048]{1,0:T(8,128)(2,1)S(1)} %convolution_convert_fusion.1), channel_id=1, source_target_pairs={{0,1},{1,0},{2,3},{3,2},{4,5},{5,4},{6,7},{7,6},{8,9},{9,8},{10,11... | collective-permute-start | bytes 589832 | tf_op jit(solution)/shard_map/ppermute | solution.py:89
  25.9 0.8 copy-start.2
  28.9 26.5 %all-to-all-start = ((bf16[64,48,128]{2,1,0:T(8,128)(2,1)}), bf16[64,48,128]{2,1,0:T(8,128)(2,1)S(1)}, u32[]{:S(2)}, u32[]{:S(2)}) async-start(bf16[64,48,128]{2,1,0:T(8,128)(2,1)} %reshape.224), calls=%async_computation | async-start | bytes 1572864 | tf_op jit(solution)/shard_map/all_to_all | solution.py:112
  40.2 20.5 %collective-permute-start.1 = (bf16[2048,256]{1,0:T(8,128)(2,1)}, bf16[2048,256]{1,0:T(8,128)(2,1)}, u32[]{:S(2)}, u32[]{:S(2)}) collective-permute-start(bf16[2048,256]{1,0:T(8,128)(2,1)} %bitcast.60), channel_id=1, source_target_pairs={{0,1},{1,0},{2,3},{3,2},{4,5},{5,4},{6,7},{7,6},{8,9},{9,8},{10,11... | collective-permute-start | bytes 3145736 | tf_op jit(solution)/shard_map/ppermute | solution.py:99
  40.9 22.1 %collective-permute-start.2 = (bf16[2048,256]{1,0:T(8,128)(2,1)}, bf16[2048,256]{1,0:T(8,128)(2,1)}, u32[]{:S(2)}, u32[]{:S(2)}) collective-permute-start(bf16[2048,256]{1,0:T(8,128)(2,1)} %bitcast.61), channel_id=1, source_target_pairs={{0,1},{1,0},{2,3},{3,2},{4,5},{5,4},{6,7},{7,6},{8,9},{9,8},{10,11... | collective-permute-start | bytes 3145736 | tf_op jit(solution)/shard_map/ppermute | solution.py:99
  41.0 22.0 %collective-permute-start.3 = (bf16[256,2048]{1,0:T(8,128)(2,1)}, bf16[256,2048]{1,0:T(8,128)(2,1)}, u32[]{:S(2)}, u32[]{:S(2)}) collective-permute-start(bf16[256,2048]{1,0:T(8,128)(2,1)} %bitcast.62), channel_id=1, source_target_pairs={{0,1},{1,0},{2,3},{3,2},{4,5},{5,4},{6,7},{7,6},{8,9},{9,8},{10,11... | collective-permute-start | bytes 3145736 | tf_op jit(solution)/shard_map/ppermute | solution.py:99
  68.8 19.2 %copy-start.9 = (f32[48,4]{0,1:T(4,128)S(1)}, f32[48,4]{0,1:T(4,128)}, u32[]{:S(2)}) copy-start(f32[48,4]{0,1:T(4,128)} %param.30) | copy-start | bytes 2308
  68.8 18.8 %all-to-all-start.1 = ((bf16[64,48,128]{2,1,0:T(8,128)(2,1)}), bf16[64,48,128]{2,1,0:T(8,128)(2,1)S(1)}, u32[]{:S(2)}, u32[]{:S(2)}) async-start(bf16[64,48,128]{2,1,0:T(8,128)(2,1)} %reshape.226), calls=%async_computation.1 | async-start | bytes 1572864 | tf_op jit(solution)/shard_map/all_to_all | solution.py:124
  73.7 18.8 %copy-start.3 = (f32[48,2048]{1,0:T(8,128)S(1)}, f32[48,2048]{1,0:T(8,128)}, u32[]{:S(2)}) copy-start(f32[48,2048]{1,0:T(8,128)} %copy-done.2) | copy-start | bytes 1179652
  88.4 4.2 %collective-permute-start.4 = (f32[48,1024]{1,0:T(8,128)S(1)}, f32[48,1024]{1,0:T(8,128)S(1)}, u32[]{:S(2)}, u32[]{:S(2)}) collective-permute-start(f32[48,1024]{1,0:T(8,128)S(1)} %constant_dynamic-slice_fusion), channel_id=1, source_target_pairs={{0,1},{1,0},{2,3},{3,2},{4,5},{5,4},{6,7},{7,6},{8,9},{9,8},{10,11... | collective-permute-start | bytes 589832 | tf_op jit(solution)/shard_map/ppermute | solution.py:132

commit v2 on v1

v2 whole, which is shorter than its diff:
```python
import functools
import jax
import jax.numpy as jnp
from jax import lax
from jax.experimental import pallas as pl
from jax.experimental.pallas import tpu as pltpu
from jax.sharding import PartitionSpec as P

EPS = 1e-06
LANES = 128
GROUP = 8
F32, BF16 = jnp.float32, jnp.bfloat16


def dot(a, b):
    return jnp.dot(a, b, preferred_element_type=F32)


def dot_nt(a, b):
    return lax.dot_general(a, b, (((1,), (1,)), ((), ())), preferred_element_type=F32)


def scaled_rows(flt, gain):
    scale = lax.rsqrt(jnp.mean(flt * flt, axis=-1, keepdims=True) + EPS)
    blocks = [
        flt[:, j * LANES : (j + 1) * LANES] * scale * gain[j : j + 1, :]
        for j in range(gain.shape[0])
    ]
    return jnp.concatenate(blocks, axis=1).astype(BF16)


def attention_kernel(
    share, lengths, core, tokens_hbm, gain_hbm, wq_hbm, wk_hbm, wv_hbm, forget_hbm, wo_hbm,
    keys_hbm, values_hbm, gates_hbm, routes_hbm, partial_ref, slots_ref,
    tokens, gain, wq, wk, wv, forget, wo, keys, values, gates, routes, attended,
    small_sems, key_sems, value_sems,
):
    seqs, places, head = keys.shape
    small = [
        (tokens_hbm, tokens), (gain_hbm, gain), (wq_hbm, wq), (wk_hbm, wk), (wv_hbm, wv),
        (forget_hbm, forget), (gates_hbm, gates), (routes_hbm, routes), (wo_hbm, wo),
    ]
    copies = [pltpu.make_async_copy(a, b, small_sems.at[i]) for i, (a, b) in enumerate(small)]

    def cached(hbm, vmem, sems, s):
        filled = pl.multiple_of((lengths[s] + LANES - 1) // LANES * LANES, LANES)
        return pltpu.make_async_copy(
            hbm.at[s, pl.ds(0, filled)], vmem.at[s, pl.ds(0, filled)], sems.at[s]
        )

    for c in copies[:-1]:
        c.start()
    groups = seqs // GROUP

    def each(action, hbm, vmem, sems, g):
        for s in range(g * GROUP, (g + 1) * GROUP):
            getattr(cached(hbm, vmem, sems, s), action)()

    each("start", keys_hbm, keys, key_sems, 0)
    each("start", keys_hbm, keys, key_sems, 1)

    def clear(s, _):
        values[s] = jnp.zeros((places, head), BF16)
        return 0

    lax.fori_loop(0, seqs, clear, 0)
    for g in range(groups):
        each("start", values_hbm, values, value_sems, g)
        if g + 2 < groups:
            each("start", keys_hbm, keys, key_sems, g + 2)
    copies[-1].start()
    for c in copies[:-1]:
        c.wait()

    named = routes[...]
    top, n_exp = named.shape[0], 64
    expert = lax.broadcasted_iota(jnp.int32, (n_exp, seqs), 0)
    hits = [expert == named[k : k + 1, :] for k in range(top)]
    onehot = sum(h.astype(F32) for h in hits)
    before = lax.broadcasted_iota(jnp.int32, (seqs, seqs), 0) < lax.broadcasted_iota(
        jnp.int32, (seqs, seqs), 1
    )
    count = dot(onehot.astype(BF16), before.astype(BF16))
    for k in range(top):
        rank = jnp.sum(jnp.where(hits[k], count, 0.0), axis=0, keepdims=True).astype(jnp.int32)
        rank = rank - core[0] * share
        mine = (rank >= 0) & (rank < share)
        slots_ref[k : k + 1, :] = jnp.where(mine, named[k : k + 1, :] * share + rank, -1)

    normed = scaled_rows(tokens[...].astype(F32), gain[...].astype(F32))
    query = dot(normed, wq[...]).astype(BF16)
    key_new = dot(normed, wk[...]).astype(BF16).astype(F32)
    value_new = dot(normed, wv[...]).astype(BF16).astype(F32)
    raw = dot_nt(normed, forget[...])
    column = lax.broadcasted_iota(jnp.int32, raw.shape, 1) == core[0]
    raw = jnp.sum(jnp.where(column, raw, 0.0), axis=1, keepdims=True)
    log_forget = jnp.minimum(raw, 0.0) - jnp.log1p(jnp.exp(-jnp.abs(raw)))

    scale = head ** (-0.5)
    rows2 = lax.broadcasted_iota(jnp.int32, (2 * GROUP, 1), 0) % GROUP
    rows1 = lax.broadcasted_iota(jnp.int32, (GROUP, 1), 0)
    place = lax.broadcasted_iota(jnp.int32, (GROUP, places), 1)

    def scores_of(g):
        own_rows = slice(g * GROUP, (g + 1) * GROUP)
        q_two = jnp.concatenate([query[own_rows, :head], query[own_rows, head:]], axis=0)
        raw_scores = jnp.zeros((2 * GROUP, places), F32)
        for i in range(GROUP):
            raw_scores = jnp.where(
                rows2 == i, dot_nt(q_two, keys[g * GROUP + i]), raw_scores
            )
        return q_two, raw_scores

    def probs_of(g, q_two, raw_scores):
        own_rows = slice(g * GROUP, (g + 1) * GROUP)
        size = jnp.zeros((GROUP, 1), jnp.int32)
        for i in range(GROUP):
            size = jnp.where(rows1 == i, lengths[g * GROUP + i], size)
        steps = places // LANES
        cum = jnp.concatenate(
            [gates[pl.ds(g * GROUP * steps + j, GROUP, stride=steps), :] for j in range(steps)],
            axis=1,
        )
        last = jnp.sum(jnp.where(place == size - 1, cum, 0.0), axis=1, keepdims=True)
        bias = (log_forget[own_rows] + last) - cum
        valid = place < size
        both = jnp.concatenate([bias, bias], axis=0)
        keep = jnp.concatenate([size, size], axis=0)
        scores = raw_scores * scale + both
        place2 = lax.broadcasted_iota(jnp.int32, (2 * GROUP, places), 1)
        scores = jnp.where(place2 < keep, scores, -jnp.inf)
        k_two = jnp.concatenate([key_new[own_rows], key_new[own_rows]], axis=0)
        own = jnp.sum(q_two.astype(F32) * k_two, axis=1, keepdims=True) * scale
        peak = jnp.maximum(jnp.max(scores, axis=1, keepdims=True), own)
        expo = jnp.exp(scores - peak)
        own_expo = jnp.exp(own - peak)
        denom = jnp.sum(expo, axis=1, keepdims=True) + own_expo
        inverse = 1.0 / denom
        probs = (expo * inverse).astype(BF16)
        own_prob = (own_expo * inverse).astype(BF16).astype(F32)
        v_two = jnp.concatenate([value_new[own_rows], value_new[own_rows]], axis=0)
        return probs, own_prob * v_two

    def result_of(g, probs, own):
        result = jnp.zeros((2 * GROUP, head), F32)
        for i in range(GROUP):
            result = jnp.where(rows2 == i, dot(probs, values[g * GROUP + i]), result)
        result = (result + own).astype(BF16)
        own_rows = slice(g * GROUP, (g + 1) * GROUP)
        attended[own_rows, :head] = result[:GROUP]
        attended[own_rows, head:] = result[GROUP:]

    each("wait", keys_hbm, keys, key_sems, 0)
    pending = scores_of(0)
    for g in range(groups):
        each("wait", values_hbm, values, value_sems, g)
        if g + 1 < groups:
            each("wait", keys_hbm, keys, key_sems, g + 1)
        probs, own = probs_of(g, *pending)
        if g + 1 < groups:
            pending = scores_of(g + 1)
        result_of(g, probs, own)
    copies[-1].wait()
    partial_ref[...] = dot(attended[...], wo[...]).astype(BF16)


def attention(share, tokens, gain, wq, wk, wv, forget, wo, keys, values, gates, lengths, routes, core):
    seqs, places, head = keys.shape
    anywhere = pl.BlockSpec(memory_space=pl.ANY)
    scalar = pl.BlockSpec(memory_space=pltpu.SMEM)
    inputs = (tokens, gain, wq, wk, wv, forget, wo, keys, values, gates, routes)
    order = (tokens, gain, wq, wk, wv, forget, wo, keys, values, gates, routes)
    return pl.pallas_call(
        functools.partial(attention_kernel, share),
        out_shape=(
            jax.ShapeDtypeStruct(tokens.shape, BF16),
            jax.ShapeDtypeStruct(routes.shape, jnp.int32),
        ),
        in_specs=[scalar, scalar] + [anywhere] * len(inputs),
        out_specs=(pl.BlockSpec(memory_space=pltpu.VMEM), pl.BlockSpec(memory_space=pltpu.VMEM)),
        scratch_shapes=[pltpu.VMEM(a.shape, a.dtype) for a in order]
        + [
            pltpu.VMEM((seqs, wo.shape[0]), BF16),
            pltpu.SemaphoreType.DMA((9,)),
            pltpu.SemaphoreType.DMA((seqs,)),
            pltpu.SemaphoreType.DMA((seqs,)),
        ],
        compiler_params=pltpu.CompilerParams(vmem_limit_bytes=56 << 20),
        name="attention",
    )(lengths, core, *inputs)


def dispatch_kernel(
    tokens_ref, own_ref, peer_ref, gain_ref, slots_any, send_ref, resid_ref, wide, rows, slots, sem
):
    top, seqs = slots.shape
    copy = pltpu.make_async_copy(slots_any, slots, sem)
    copy.start()
    mixed = own_ref[...].astype(F32) + peer_ref[...].astype(F32)
    resid = (tokens_ref[...].astype(F32) + mixed).astype(BF16)
    resid_ref[...] = resid
    expert_in = scaled_rows(resid.astype(F32), gain_ref[...].astype(F32)).astype(F32)
    for j in range(wide.shape[1]):
        wide[:, j, :] = expert_in[:, j * LANES : (j + 1) * LANES]
    used = send_ref.shape[0]
    copy.wait()
    for t in range(seqs):
        row = wide[t].astype(BF16)
        for k in range(top):
            slot = slots[k, t]
            rows[jnp.where(slot < 0, used, slot)] = row
    send_ref[...] = rows[:used]


def dispatch(used, tokens, own, peer, gain, slots):
    seqs, width = tokens.shape
    blocks = width // LANES
    vmem = pl.BlockSpec(memory_space=pltpu.VMEM)
    return pl.pallas_call(
        dispatch_kernel,
        out_shape=(
            pltpu.VMEM((used, blocks, LANES), BF16),
            pltpu.VMEM((seqs, width), BF16),
        ),
        in_specs=[vmem] * 4 + [SLOTS_SPEC],
        out_specs=(vmem, vmem),
        scratch_shapes=[
            pltpu.VMEM((seqs, blocks, LANES), F32),
            pltpu.VMEM((used + 8, blocks, LANES), BF16),
            pltpu.SMEM(slots.shape, jnp.int32),
            pltpu.SemaphoreType.DMA,
        ],
        name="dispatch",
    )(tokens, own, peer, gain, slots)


def experts_kernel(
    rows_ref, gate_own, up_own, down_own, gate_peer, up_peer, down_peer, out_ref, wide
):
    blocks = wide.shape[1]
    wide[...] = rows_ref[...].astype(F32)
    rows = jnp.concatenate([wide[:, j, :].astype(BF16) for j in range(blocks)], axis=1)

    def hidden(gate_w, up_w):
        gate = dot(rows, gate_w[...])
        return (gate / (1.0 + jnp.exp(-gate)) * dot(rows, up_w[...])).astype(BF16)

    act = jnp.concatenate([hidden(gate_own, up_own), hidden(gate_peer, up_peer)], axis=1)
    down = jnp.concatenate([down_own[...], down_peer[...]], axis=0)
    outputs = dot(act, down)
    for j in range(blocks):
        wide[:, j, :] = outputs[:, j * LANES : (j + 1) * LANES]
    out_ref[...] = wide[...].astype(BF16)


def experts(rows, *weights):
    vmem = pl.BlockSpec(memory_space=pltpu.VMEM)
    return pl.pallas_call(
        experts_kernel,
        out_shape=pltpu.VMEM(rows.shape, BF16),
        in_specs=[vmem] * 7,
        out_specs=vmem,
        scratch_shapes=[pltpu.VMEM(rows.shape, F32)],
        compiler_params=pltpu.CompilerParams(vmem_limit_bytes=40 << 20),
        name="experts",
    )(rows, *weights)


def combine_kernel(
    core, shares_any, slots_any, returned_ref, resid_ref, keep_ref, give_ref, wide, shares, slots, sems
):
    top, seqs = slots.shape
    copies = [
        pltpu.make_async_copy(slots_any, slots, sems.at[0]),
        pltpu.make_async_copy(shares_any, shares, sems.at[1]),
    ]
    for c in copies:
        c.start()
    for c in copies:
        c.wait()
    for t in range(seqs):
        total = jnp.zeros(wide.shape[1:], F32)
        for k in range(top):
            slot = slots[k, t]
            row = returned_ref[jnp.maximum(slot, 0)].astype(F32)
            total = total + jnp.where(slot >= 0, row * shares[k, t], 0.0)
        wide[t] = total
    half = wide.shape[1] // 2
    width = half * LANES
    mine = core[0]

    def columns(which):
        return jnp.concatenate([wide[:, which * half + j, :] for j in range(half)], axis=1)

    resid = jnp.where(mine == 0, resid_ref[:, :width], resid_ref[:, width:])
    keep_ref[...] = columns(mine) + resid.astype(F32)
    give_ref[...] = columns(1 - mine)


def combine(returned, slots, shares, resid, core):
    seqs, width = resid.shape
    blocks = width // LANES
    vmem = pl.BlockSpec(memory_space=pltpu.VMEM)
    half = pltpu.VMEM((seqs, width // 2), F32)
    return pl.pallas_call(
        combine_kernel,
        out_shape=(half, half),
        in_specs=[pl.BlockSpec(memory_space=pltpu.SMEM), SLOTS_SPEC, SLOTS_SPEC, vmem, vmem],
        out_specs=(vmem, vmem),
        scratch_shapes=[
            pltpu.VMEM((seqs, blocks, LANES), F32),
            pltpu.SMEM(shares.shape, F32),
            pltpu.SMEM(slots.shape, jnp.int32),
            pltpu.SemaphoreType.DMA((2,)),
        ],
        name="combine",
    )(core, shares, slots, returned, resid)


SLOTS_SPEC = pl.BlockSpec(memory_space=pl.ANY)


def shards(
    tokens, norm_gain, expert_gain, w_query, key_weight, value_weight, forget_weight, w_out,
    key_cache, cached_values, cum_gates, lengths, routes, route_weights, expert_gate, expert_up,
    expert_down,
):
    seqs, width = tokens.shape
    places, head = key_cache.shape[1], key_cache.shape[3]
    n_exp = expert_gate.shape[0] * lax.axis_size("ep")
    share = max(2, 2 * seqs * routes.shape[1] // n_exp) // 2
    used, blocks = n_exp * share, width // LANES
    swap = [(0, 1), (1, 0)]
    core = lax.axis_index("tp").reshape(1)
    own, slots = attention(
        share, tokens, norm_gain.reshape(blocks, LANES), w_query, key_weight, value_weight,
        forget_weight.T, w_out, key_cache.reshape(seqs, places, head),
        cached_values.reshape(seqs, places, head), cum_gates.reshape(-1, LANES), lengths,
        routes.T, core,
    )
    peer = lax.ppermute(own, "tp", swap)
    weights = (expert_gate[0], expert_up[0], expert_down[0])
    other = tuple(lax.ppermute(w, "tp", swap) for w in weights)
    send, resid = dispatch(used, tokens, own, peer, expert_gain.reshape(blocks, LANES), slots)

    def exchange(rows):
        slabs = rows.reshape(n_exp, share * blocks, LANES)
        slabs = lax.all_to_all(slabs, "ep", split_axis=0, concat_axis=0, tiled=True)
        return slabs.reshape(used, blocks, LANES)

    outputs = experts(exchange(send), *weights, *other)
    keep, give = combine(exchange(outputs), slots, route_weights.T, resid, core)
    got = lax.ppermute(give, "tp", swap)
    return (keep + got).astype(BF16)


def solution(mesh):
    in_specs = (
        P("ep", None),
        P(),
        P(),
        P(None, "tp"),
        P(None, "tp"),
        P(None, "tp"),
        P(),
        P("tp", None),
        P("ep", None, "tp", None),
        P("ep", None, "tp", None),
        P("ep", "tp", None),
        P("ep"),
        P("ep", None),
        P("ep", None),
        P("ep", None, "tp"),
        P("ep", None, "tp"),
        P("ep", "tp", None),
    )
    out_specs = P("ep", "tp")
    return jax.shard_map(shards, mesh=mesh, in_specs=in_specs, out_specs=out_specs, check_vma=False)
```

time: 93.8 us -> 78.8 us (0.84)
  blocking collectives: 0 us -> 45.4 us
  matrix products: 27.9 us -> 0 us
  waiting for transfers between devices: 29.6 us -> 2.72 us
  Pallas kernels: 0 us -> 22.8 us
  starting transfers between devices: 21.8 us -> 4.92 us
  other arithmetic: 7.91 us -> 0.66 us
  local copies, waits for them, and re-layouts: 5.7 us -> 1.91 us
    all_to_all x0 -> x2, blocking collectives: none -> 45.4 us  [exchange(): slabs = lax.all_to_all(slabs, 'ep', split_axis=0, concat_axis=0, tiled=True)]
    dot_general x14 -> x0, matrix products: 27.9 us -> none  [the longest x1 8.07 us: attend(): jnp.einsum('skgd,slkd->skgl', q_four, key_cache, preferred_element_type=j...]
    all_to_all x2 -> x0, waiting for transfers between devices: 27.9 us -> none  [the longest x1 14 us: shards(): lax.all_to_all(send, 'ep', split_axis=0, concat_axis=0, tiled=True)]
    pallas_call x0 -> x4, Pallas kernels: none -> 22.8 us  [the longest x1 12.7 us: attention(): pl.pallas_call(functools.partial(attention_kernel, share), out_shape=(jax...]
    all_to_all x2 -> x0, starting transfers between devices: 16 us -> none  [the longest x1 11.3 us: shards(): lax.all_to_all(send, 'ep', split_axis=0, concat_axis=0, tiled=True)]
    reshape x5 -> x0, local copies, waits for them, and re-layouts: 4.25 us -> none  [the longest x1 2.17 us: shards(): outputs.astype(jnp.bfloat16).reshape(n_exp, share * width // 128, 128)]
    reduce_sum x5 -> x0, other arithmetic: 3.57 us -> none  [the longest x1 1.68 us: attend(): jnp.sum(jnp.where(places[None, None, :] == (lengths - 1)[:, None, None],...]
    sub x2 -> x0, other arithmetic: 1.94 us -> none  [the longest x1 1.13 us: attend(): bias = (log_forget + last)[:, :, None] - cum_gates]
  transfers between devices with their start and end apart: 7 -> 5, of which waited for: 4 -> 2; matrix products, arithmetic and copies ran while one was open for 9% -> 0% of each run, Pallas kernels for 0% -> 19%
where the time goes in v2:
time: 78.8 us; the launch traced here: 78.5 us
  blocking collectives  45.4 us (58%)
  Pallas kernels  22.8 us (29%)
  starting transfers between devices  4.92 us (6%)
  waiting for transfers between devices  2.72 us (3%)
  local copies, waits for them, and re-layouts  1.91 us (2%)
    all_to_all x2, blocking collectives, exchange(): slabs = lax.all_to_all(slabs, 'ep', split_axis=0, concat_axis=0, tiled=True)  45.4 us
    pallas_call x1, Pallas kernels, attention(): pl.pallas_call(functools.partial(attention_kernel, share), out_shape=(jax...  12.7 us
    pallas_call x1, Pallas kernels, experts(): pl.pallas_call(experts_kernel, out_shape=pltpu.VMEM(rows.shape, BF16), in...  5.31 us
    ppermute x1, starting transfers between devices, shards(): got = lax.ppermute(give, 'tp', swap)  2.95 us
    pallas_call x1, Pallas kernels, combine(): pl.pallas_call(combine_kernel, out_shape=(half, half), in_specs=[pl.Block...  2.59 us
    pallas_call x1, Pallas kernels, dispatch(): pl.pallas_call(dispatch_kernel, out_shape=(pltpu.VMEM((used, blocks, LANE...  2.21 us
    unnamed x10, local copies, waits for them, and re-layouts  1.91 us
    ppermute x3, starting transfers between devices, shards(): other = tuple((lax.ppermute(w, 'tp', swap) for w in weights))  1.89 us
  transfers between devices with their start and end apart: 5, of which 2 were waited for; matrix products, arithmetic and copies ran while one was open for 0% of the time, Pallas kernels for 19%

profile of v2, /device:TPU:1, one launch (start us, length us, event | category | flops | bytes accessed | tf_op | source)
XLA Modules:
  0.0 78.5 jit_solution(11181878746162771892)
XLA Ops:
  0.0 1.4 %collective-permute-start.1 = (bf16[2048,256]{1,0:T(8,128)(2,1)}, bf16[2048,256]{1,0:T(8,128)(2,1)}, u32[]{:S(2)}, u32[]{:S(2)}) collective-permute-start(bf16[2048,256]{1,0:T(8,128)(2,1)} %bitcast.18), channel_id=1, source_target_pairs={{0,1},{1,0},{2,3},{3,2},{4,5},{5,4},{6,7},{7,6},{8,9},{9,8},{10,11... | collective-permute-start | bytes 3145736 | tf_op jit(solution)/shard_map/ppermute | solution.py:343
  1.4 0.0 collective-permute-start.2
  1.4 0.5 collective-permute-start.3
  1.9 0.0 copy-start
  1.9 0.0 copy-start.1
  1.9 12.7 %attention.1 = (bf16[48,2048]{1,0:T(8,128)(2,1)}, s32[4,48]{1,0:T(4,128)}) custom-call(s32[48]{0:T(128)} %lengths.1, s32[1]{0:T(128)} %bitcast.core, bf16[48,2048]{1,0:T(8,128)(2,1)} %tokens_ref.1, bf16[16,128]{1,0:T(8,128)(2,1)} %bitcast.31, bf16[2048,256]{1,0:T(8,128)(2,1)} %wq_hbm.1, bf16[2048,128]{1,0:T(8,128)(2,1)} %wk_hbm.1, bf16[2048,128]{1,0:T(8,128)(2,1)} %wv_hbm.1, ...), custom_call_target="tpu_custom_call" | custom-call | tf_op jit(solution)/shard_map/attention/pallas_call | solution.py:173
  14.6 0.1 collective-permute-start
  14.7 1.6 %collective-permute-done.peer_ref = bf16[48,2048]{1,0:T(8,128)(2,1)S(1)} collective-permute-done((bf16[48,2048]{1,0:T(8,128)(2,1)}, bf16[48,2048]{1,0:T(8,128)(2,1)S(1)}, u32[]{:S(2)}, u32[]{:S(2)}) %collective-permute-start) | collective-permute-done | bytes 196640 | tf_op jit(solution)/shard_map/ppermute | solution.py:341
  16.3 0.0 copy-start.4
  16.3 0.7 copy-done.4
  17.0 2.2 %dispatch.1 = (bf16[192,16,128]{2,1,0:T(8,128)(2,1)S(1)}, bf16[48,2048]{1,0:T(8,128)(2,1)S(1)}) custom-call(bf16[48,2048]{1,0:T(8,128)(2,1)} %tokens_ref.1, bf16[48,2048]{1,0:T(8,128)(2,1)} %get-tuple-element.12.own_ref, bf16[48,2048]{1,0:T(8,128)(2,1)} %copy-done.4, bf16[16,128]{1,0:T(8,128)(2,1)} %bitcast.30, s32[4,48]{1,0:T(4,128)} %get-tuple-element.11.slots_any), custom_call_target="tpu_custom_call" | custom-call | tf_op jit(solution)/shard_map/dispatch/pallas_call | solution.py:219
  19.2 0.0 copy-start.3
  19.2 26.7 %all_to_all.10 = bf16[64,48,128]{2,1,0:T(8,128)(2,1)S(1)} all-to-all(bf16[64,48,128]{2,1,0:T(8,128)(2,1)S(1)} %bitcast.24), channel_id=1, replica_groups=mesh['ep'=64,'tp'=2] {'ep'}, dimensions={0} | all-to-all | bytes 1572864 | tf_op jit(solution)/shard_map/all_to_all | solution.py:348
  45.9 0.0 collective-permute-done.1.gate_peer
  45.9 0.0 collective-permute-done.2.up_peer
  45.9 0.0 collective-permute-done.3.down_peer
  45.9 0.0 copy-done
  45.9 0.0 copy-done.1
  45.9 0.0 copy-start.2
  45.9 1.2 %copy-done.2 = bf16[1,256,2048]{2,1,0:T(8,128)(2,1)S(1)} copy-done((bf16[1,256,2048]{2,1,0:T(8,128)(2,1)S(1)}, bf16[1,256,2048]{2,1,0:T(8,128)(2,1)}, u32[]{:S(2)}) %copy-start.2) | copy-done | bytes 1048600
  47.2 5.3 %experts.1 = bf16[192,16,128]{2,1,0:T(8,128)(2,1)S(1)} custom-call(bf16[192,16,128]{2,1,0:T(8,128)(2,1)S(1)} %bitcast.16, bf16[2048,256]{1,0:T(8,128)(2,1)S(1)} %bitcast.19, bf16[2048,256]{1,0:T(8,128)(2,1)S(1)} %bitcast.21, bf16[256,2048]{1,0:T(8,128)(2,1)S(1)} %bitcast.23, bf16[2048,256]{1,0:T(8,128)(2,1)} %collective-permute-done.1.gate_peer, ...), custom_call_target="tpu_custom_call" | custom-call | tf_op jit(solution)/shard_map/experts/pallas_call | solution.py:258
  52.5 18.7 %all_to_all.11 = bf16[64,48,128]{2,1,0:T(8,128)(2,1)} all-to-all(bf16[64,48,128]{2,1,0:T(8,128)(2,1)S(1)} %bitcast.17), channel_id=1, replica_groups=mesh['ep'=64,'tp'=2] {'ep'}, dimensions={0} | all-to-all | bytes 1572864 | tf_op jit(solution)/shard_map/all_to_all | solution.py:348
  71.2 0.0 copy-done.3
  71.2 2.6 %combine.1 = (f32[48,1024]{1,0:T(8,128)S(1)}, f32[48,1024]{1,0:T(8,128)S(1)}) custom-call(s32[1]{0:T(128)} %bitcast.core, f32[4,48]{1,0:T(4,128)} %bitcast.32, s32[4,48]{1,0:T(4,128)} %get-tuple-element.11.slots_any, bf16[192,16,128]{2,1,0:T(8,128)(2,1)} %bitcast.27, bf16[48,2048]{1,0:T(8,128)(2,1)} %copy-done.3), custom_call_target="tpu_custom_call" | custom-call | tf_op jit(solution)/shard_map/combine/pallas_call | solution.py:305
  73.8 2.9 %collective-permute-start.4 = (f32[48,1024]{1,0:T(8,128)S(1)}, f32[48,1024]{1,0:T(8,128)S(1)}, u32[]{:S(2)}, u32[]{:S(2)}) collective-permute-start(f32[48,1024]{1,0:T(8,128)S(1)} %get-tuple-element.16), channel_id=1, source_target_pairs={{0,1},{1,0},{2,3},{3,2},{4,5},{5,4},{6,7},{7,6},{8,9},{9,8},{10,11... | collective-permute-start | bytes 589832 | tf_op jit(solution)/shard_map/ppermute | solution.py:353
  76.7 1.1 %collective-permute-done.4 = f32[48,1024]{1,0:T(8,128)S(1)} collective-permute-done((f32[48,1024]{1,0:T(8,128)S(1)}, f32[48,1024]{1,0:T(8,128)S(1)}, u32[]{:S(2)}, u32[]{:S(2)}) %collective-permute-start.4) | collective-permute-done | bytes 196640 | tf_op jit(solution)/shard_map/ppermute | solution.py:353
  77.8 0.7 add_convert_fusion
Async XLA Ops:
  0.0 45.9 %collective-permute-start.1 = (bf16[2048,256]{1,0:T(8,128)(2,1)}, bf16[2048,256]{1,0:T(8,128)(2,1)}, u32[]{:S(2)}, u32[]{:S(2)}) collective-permute-start(bf16[2048,256]{1,0:T(8,128)(2,1)} %bitcast.18), channel_id=1, source_target_pairs={{0,1},{1,0},{2,3},{3,2},{4,5},{5,4},{6,7},{7,6},{8,9},{9,8},{10,11... | collective-permute-start | bytes 3145736 | tf_op jit(solution)/shard_map/ppermute | solution.py:343
  1.4 44.5 %collective-permute-start.2 = (bf16[2048,256]{1,0:T(8,128)(2,1)}, bf16[2048,256]{1,0:T(8,128)(2,1)}, u32[]{:S(2)}, u32[]{:S(2)}) collective-permute-start(bf16[2048,256]{1,0:T(8,128)(2,1)} %bitcast.20), channel_id=1, source_target_pairs={{0,1},{1,0},{2,3},{3,2},{4,5},{5,4},{6,7},{7,6},{8,9},{9,8},{10,11... | collective-permute-start | bytes 3145736 | tf_op jit(solution)/shard_map/ppermute | solution.py:343
  1.4 44.5 %collective-permute-start.3 = (bf16[256,2048]{1,0:T(8,128)(2,1)}, bf16[256,2048]{1,0:T(8,128)(2,1)}, u32[]{:S(2)}, u32[]{:S(2)}) collective-permute-start(bf16[256,2048]{1,0:T(8,128)(2,1)} %bitcast.22), channel_id=1, source_target_pairs={{0,1},{1,0},{2,3},{3,2},{4,5},{5,4},{6,7},{7,6},{8,9},{9,8},{10,11... | collective-permute-start | bytes 3145736 | tf_op jit(solution)/shard_map/ppermute | solution.py:343
  1.9 44.0 %copy-start = (bf16[1,2048,256]{2,1,0:T(8,128)(2,1)S(1)}, bf16[1,2048,256]{2,1,0:T(8,128)(2,1)}, u32[]{:S(2)}) copy-start(bf16[1,2048,256]{2,1,0:T(8,128)(2,1)} %param.31) | copy-start | bytes 3145732
  1.9 44.0 %copy-start.1 = (bf16[1,2048,256]{2,1,0:T(8,128)(2,1)S(1)}, bf16[1,2048,256]{2,1,0:T(8,128)(2,1)}, u32[]{:S(2)}) copy-start(bf16[1,2048,256]{2,1,0:T(8,128)(2,1)} %param.32) | copy-start | bytes 3145732
  14.6 1.7 %collective-permute-start = (bf16[48,2048]{1,0:T(8,128)(2,1)}, bf16[48,2048]{1,0:T(8,128)(2,1)S(1)}, u32[]{:S(2)}, u32[]{:S(2)}) collective-permute-start(bf16[48,2048]{1,0:T(8,128)(2,1)} %get-tuple-element.12.own_ref), channel_id=1, source_target_pairs={{0,1},{1,0},{2,3},{3,2},{4,5},{5,4},{6,7},{7,6},{8,9},{9,8},{10,11... | collective-permute-start | bytes 589832 | tf_op jit(solution)/shard_map/ppermute | solution.py:341
  16.3 0.7 copy-start.4
  19.2 52.0 %copy-start.3 = (bf16[48,2048]{1,0:T(8,128)(2,1)}, bf16[48,2048]{1,0:T(8,128)(2,1)S(1)}, u32[]{:S(2)}) copy-start(bf16[48,2048]{1,0:T(8,128)(2,1)S(1)} %get-tuple-element.14.resid_ref) | copy-start | bytes 589828
  45.9 1.2 %copy-start.2 = (bf16[1,256,2048]{2,1,0:T(8,128)(2,1)S(1)}, bf16[1,256,2048]{2,1,0:T(8,128)(2,1)}, u32[]{:S(2)}) copy-start(bf16[1,256,2048]{2,1,0:T(8,128)(2,1)} %param.33) | copy-start | bytes 3145732
  73.8 4.0 %collective-permute-start.4 = (f32[48,1024]{1,0:T(8,128)S(1)}, f32[48,1024]{1,0:T(8,128)S(1)}, u32[]{:S(2)}, u32[]{:S(2)}) collective-permute-start(f32[48,1024]{1,0:T(8,128)S(1)} %get-tuple-element.16), channel_id=1, source_target_pairs={{0,1},{1,0},{2,3},{3,2},{4,5},{5,4},{6,7},{7,6},{8,9},{9,8},{10,11... | collective-permute-start | bytes 589832 | tf_op jit(solution)/shard_map/ppermute | solution.py:353

commit v3 on v2

--- a/solution.py
+++ b/solution.py
@@ -9,6 +9,8 @@
 EPS = 1e-06
 LANES = 128
 GROUP = 8
+CHUNK = 256
+SPANS = ((0,),(1,),(2,),(3,),(4,),(5,))
 F32, BF16 = jnp.float32, jnp.bfloat16
 
 
@@ -31,46 +33,54 @@
 
 def attention_kernel(
     share, lengths, core, tokens_hbm, gain_hbm, wq_hbm, wk_hbm, wv_hbm, forget_hbm, wo_hbm,
-    keys_hbm, values_hbm, gates_hbm, routes_hbm, partial_ref, slots_ref,
+    keys_hbm, values_hbm, gates_hbm, routes_hbm, gate_hbm, up_hbm, down_hbm, partial_ref, slots_ref,
+    gate_ref, up_ref, down_ref,
     tokens, gain, wq, wk, wv, forget, wo, keys, values, gates, routes, attended,
-    small_sems, key_sems, value_sems,
-):
-    seqs, places, head = keys.shape
+    small_sems, key_sems, value_sems, weight_sems,
+):
+    seqs = attended.shape[0]
+    places, head = keys.shape[0] // seqs, keys.shape[1]
     small = [
         (tokens_hbm, tokens), (gain_hbm, gain), (wq_hbm, wq), (wk_hbm, wk), (wv_hbm, wv),
         (forget_hbm, forget), (gates_hbm, gates), (routes_hbm, routes), (wo_hbm, wo),
     ]
     copies = [pltpu.make_async_copy(a, b, small_sems.at[i]) for i, (a, b) in enumerate(small)]
 
-    def cached(hbm, vmem, sems, s):
-        filled = pl.multiple_of((lengths[s] + LANES - 1) // LANES * LANES, LANES)
-        return pltpu.make_async_copy(
-            hbm.at[s, pl.ds(0, filled)], vmem.at[s, pl.ds(0, filled)], sems.at[s]
-        )
+    def filled(s):
+        return lax.shift_right_logical(lengths[s] + (LANES - 1), 7)
+
+    def start(hbm, vmem, sems, which):
+        for g in which:
+            for s in range(g * GROUP, (g + 1) * GROUP):
+                count = pl.multiple_of(lax.shift_left(filled(s), 7), LANES)
+                at = pl.ds(s * places, count)
+                pltpu.make_async_copy(hbm.at[at], vmem.at[at], sems.at[g]).start()
+
+    def wait(hbm, vmem, sems, which):
+        for g in which:
+            count = sum(filled(s) for s in range(g * GROUP, (g + 1) * GROUP))
+            at = pl.ds(0, pl.multiple_of(lax.shift_left(count, 7), LANES))
+            pltpu.make_async_copy(hbm.at[at], vmem.at[at], sems.at[g]).wait()
+
+    def start_values(which):
+        for g in which:
+            for s in range(g * GROUP, (g + 1) * GROUP):
+                edge = jnp.minimum(filled(s), places // LANES - 1)
+                at = pl.multiple_of(s * places + lax.shift_left(edge, 7), LANES)
+                values[pl.ds(at, LANES), :] = jnp.zeros((LANES, head), BF16)
+        start(values_hbm, values, value_sems, which)
 
     for c in copies[:-1]:
         c.start()
-    groups = seqs // GROUP
-
-    def each(action, hbm, vmem, sems, g):
-        for s in range(g * GROUP, (g + 1) * GROUP):
-            getattr(cached(hbm, vmem, sems, s), action)()
-
-    each("start", keys_hbm, keys, key_sems, 0)
-    each("start", keys_hbm, keys, key_sems, 1)
-
-    def clear(s, _):
-        values[s] = jnp.zeros((places, head), BF16)
-        return 0
-
-    lax.fori_loop(0, seqs, clear, 0)
-    for g in range(groups):
-        each("start", values_hbm, values, value_sems, g)
-        if g + 2 < groups:
-            each("start", keys_hbm, keys, key_sems, g + 2)
-    copies[-1].start()
+    spans = SPANS + ((), (), ())
+    start(keys_hbm, keys, key_sems, spans[0])
     for c in copies[:-1]:
         c.wait()
+    start(keys_hbm, keys, key_sems, spans[1])
+    start_values(spans[0])
+    start(keys_hbm, keys, key_sems, spans[2])
+    start_values(spans[1])
+    copies[-1].start()
 
     named = routes[...]
     top, n_exp = named.shape[0], 64
@@ -107,7 +117,7 @@
         raw_scores = jnp.zeros((2 * GROUP, places), F32)
         for i in range(GROUP):
             raw_scores = jnp.where(
-                rows2 == i, dot_nt(q_two, keys[g * GROUP + i]), raw_scores
+                rows2 == i, dot_nt(q_two, keys[(g * GROUP + i) * places : (g * GROUP + i + 1) * places]), raw_scores
             )
         return q_two, raw_scores
 
@@ -142,74 +152,113 @@
         return probs, own_prob * v_two
 
     def result_of(g, probs, own):
-        result = jnp.zeros((2 * GROUP, head), F32)
+        result = own
         for i in range(GROUP):
-            result = jnp.where(rows2 == i, dot(probs, values[g * GROUP + i]), result)
-        result = (result + own).astype(BF16)
+            s = g * GROUP + i
+            for c in range(0, places, CHUNK):
+                part = dot(probs[:, c : c + CHUNK], values[s * places + c : s * places + c + CHUNK])
+                used = rows2 == i
+                if c:
+                    used = used & (lengths[s] > c)
+                result = result + jnp.where(used, part, 0.0)
+        result = result.astype(BF16)
         own_rows = slice(g * GROUP, (g + 1) * GROUP)
         attended[own_rows, :head] = result[:GROUP]
         attended[own_rows, head:] = result[GROUP:]
 
-    each("wait", keys_hbm, keys, key_sems, 0)
-    pending = scores_of(0)
-    for g in range(groups):
-        each("wait", values_hbm, values, value_sems, g)
-        if g + 1 < groups:
-            each("wait", keys_hbm, keys, key_sems, g + 1)
-        probs, own = probs_of(g, *pending)
-        if g + 1 < groups:
-            pending = scores_of(g + 1)
-        result_of(g, probs, own)
+    wait(keys_hbm, keys, key_sems, spans[0])
+    pairs = [(gate_hbm, gate_ref), (up_hbm, up_ref), (down_hbm, down_ref)]
+    moved = [pltpu.make_async_copy(a, b, weight_sems.at[i]) for i, (a, b) in enumerate(pairs)]
+    pending = [scores_of(g) for g in spans[0]]
+    for i, span in enumerate(SPANS):
+        start(keys_hbm, keys, key_sems, spans[i + 3])
+        start_values(spans[i + 2])
+        if i + 3 == len(SPANS):
+            for c in moved:
+                c.start()
+        wait(values_hbm, values, value_sems, span)
+        wait(keys_hbm, keys, key_sems, spans[i + 1])
+        ready = [probs_of(g, *p) for g, p in zip(span, pending)]
+        pending = [scores_of(g) for g in spans[i + 1]]
+        for g, (probs, own) in zip(span, ready):
+            result_of(g, probs, own)
+    for c in moved:
+        c.wait()
     copies[-1].wait()
     partial_ref[...] = dot(attended[...], wo[...]).astype(BF16)
 
 
-def attention(share, tokens, gain, wq, wk, wv, forget, wo, keys, values, gates, lengths, routes, core):
-    seqs, places, head = keys.shape
+def attention(
+    share, tokens, gain, wq, wk, wv, forget, wo, keys, values, gates, lengths, routes, core, weights
+):
+    seqs = tokens.shape[0]
     anywhere = pl.BlockSpec(memory_space=pl.ANY)
+    hbm = pl.BlockSpec(memory_space=pltpu.HBM)
     scalar = pl.BlockSpec(memory_space=pltpu.SMEM)
     inputs = (tokens, gain, wq, wk, wv, forget, wo, keys, values, gates, routes)
     order = (tokens, gain, wq, wk, wv, forget, wo, keys, values, gates, routes)
     return pl.pallas_call(
         functools.partial(attention_kernel, share),
         out_shape=(
-            jax.ShapeDtypeStruct(tokens.shape, BF16),
-            jax.ShapeDtypeStruct(routes.shape, jnp.int32),
+            pltpu.VMEM(tokens.shape, BF16),
+            pltpu.VMEM(routes.shape, jnp.int32),
+            *(pltpu.VMEM(w.shape, w.dtype) for w in weights),
         ),
-        in_specs=[scalar, scalar] + [anywhere] * len(inputs),
-        out_specs=(pl.BlockSpec(memory_space=pltpu.VMEM), pl.BlockSpec(memory_space=pltpu.VMEM)),
+        in_specs=[scalar, scalar] + [anywhere] * len(inputs) + [hbm] * len(weights),
+        out_specs=[pl.BlockSpec(memory_space=pltpu.VMEM)] * (2 + len(weights)),
         scratch_shapes=[pltpu.VMEM(a.shape, a.dtype) for a in order]
         + [
             pltpu.VMEM((seqs, wo.shape[0]), BF16),
             pltpu.SemaphoreType.DMA((9,)),
-            pltpu.SemaphoreType.DMA((seqs,)),
-            pltpu.SemaphoreType.DMA((seqs,)),
+            pltpu.SemaphoreType.DMA((seqs // GROUP,)),
+            pltpu.SemaphoreType.DMA((seqs // GROUP,)),
+            pltpu.SemaphoreType.DMA((len(weights),)),
         ],
-        compiler_params=pltpu.CompilerParams(vmem_limit_bytes=56 << 20),
+        compiler_params=pltpu.CompilerParams(vmem_limit_bytes=52 << 20),
         name="attention",
-    )(lengths, core, *inputs)
+    )(lengths, core, *inputs, *(far(w) for w in weights))
+
+
+def swapped(blocks):
+    size = blocks * blocks
+    first = lax.broadcasted_iota(jnp.int32, (size, size), 0)
+    second = lax.broadcasted_iota(jnp.int32, (size, size), 1)
+    same = (first // blocks == second % blocks) & (first % blocks == second // blocks)
+    return same.astype(F32).astype(BF16)
+
+
+def stacked(values, first, blocks):
+    rows = values[first : first + blocks]
+    return jnp.concatenate([rows[:, j * LANES : (j + 1) * LANES] for j in range(blocks)], axis=0)
 
 
 def dispatch_kernel(
-    tokens_ref, own_ref, peer_ref, gain_ref, slots_any, send_ref, resid_ref, wide, rows, slots, sem
+    tokens_ref, own_ref, peer_ref, gain_ref, slots_any, send_ref, resid_ref, lines, slots, sem
 ):
     top, seqs = slots.shape
     copy = pltpu.make_async_copy(slots_any, slots, sem)
     copy.start()
+    blocks = gain_ref.shape[0]
     mixed = own_ref[...].astype(F32) + peer_ref[...].astype(F32)
     resid = (tokens_ref[...].astype(F32) + mixed).astype(BF16)
     resid_ref[...] = resid
-    expert_in = scaled_rows(resid.astype(F32), gain_ref[...].astype(F32)).astype(F32)
-    for j in range(wide.shape[1]):
-        wide[:, j, :] = expert_in[:, j * LANES : (j + 1) * LANES]
+    expert_in = scaled_rows(resid.astype(F32), gain_ref[...].astype(F32))
     used = send_ref.shape[0]
+    lines[...] = jnp.zeros(lines.shape, BF16)
+    turn = swapped(blocks)
+    by_token = [
+        dot(turn, stacked(expert_in, first, blocks)).astype(BF16)
+        for first in range(0, seqs, blocks)
+    ]
     copy.wait()
     for t in range(seqs):
-        row = wide[t].astype(BF16)
+        start = t % blocks * blocks
+        row = by_token[t // blocks][start : start + blocks]
         for k in range(top):
             slot = slots[k, t]
-            rows[jnp.where(slot < 0, used, slot)] = row
-    send_ref[...] = rows[:used]
+            place = jnp.where(slot < 0, used, slot * blocks)
+            lines[pl.ds(pl.multiple_of(place, blocks), blocks), :] = row
+    send_ref[...] = lines[:used]
 
 
 def dispatch(used, tokens, own, peer, gain, slots):
@@ -218,52 +267,63 @@
     vmem = pl.BlockSpec(memory_space=pltpu.VMEM)
     return pl.pallas_call(
         dispatch_kernel,
-        out_shape=(
-            pltpu.VMEM((used, blocks, LANES), BF16),
-            pltpu.VMEM((seqs, width), BF16),
-        ),
+        out_shape=(pltpu.VMEM((used * blocks, LANES), BF16), pltpu.VMEM((seqs, width), BF16)),
         in_specs=[vmem] * 4 + [SLOTS_SPEC],
         out_specs=(vmem, vmem),
         scratch_shapes=[
-            pltpu.VMEM((seqs, blocks, LANES), F32),
-            pltpu.VMEM((used + 8, blocks, LANES), BF16),
+            pltpu.VMEM(((used + 1) * blocks, LANES), BF16),
             pltpu.SMEM(slots.shape, jnp.int32),
             pltpu.SemaphoreType.DMA,
         ],
+        compiler_params=pltpu.CompilerParams(vmem_limit_bytes=16 << 20),
         name="dispatch",
-    )(tokens, own, peer, gain, slots)
+    )(near(tokens), near(own), near(peer), near(gain), near(slots))
 
 
 def experts_kernel(
-    rows_ref, gate_own, up_own, down_own, gate_peer, up_peer, down_peer, out_ref, wide
-):
-    blocks = wide.shape[1]
-    wide[...] = rows_ref[...].astype(F32)
-    rows = jnp.concatenate([wide[:, j, :].astype(BF16) for j in range(blocks)], axis=1)
+    lines_ref, gate_own, up_own, down_own, gate_peer, up_peer, down_peer, out_ref, rows
+):
+    count, width = rows.shape
+    blocks = width // LANES
+    size = blocks * blocks
+    turn = swapped(blocks)
+    for first in range(0, count, 2 * blocks):
+        at = first * blocks
+        both = [lines_ref[at : at + size], lines_ref[at + size : at + 2 * size]]
+        turned = dot(turn, jnp.concatenate(both, axis=1)).astype(BF16)
+        for i in range(2):
+            start = first + i * blocks
+            for j in range(blocks):
+                rows[start : start + blocks, j * LANES : (j + 1) * LANES] = turned[
+                    j * blocks : (j + 1) * blocks, i * LANES : (i + 1) * LANES
+                ]
 
     def hidden(gate_w, up_w):
-        gate = dot(rows, gate_w[...])
-        return (gate / (1.0 + jnp.exp(-gate)) * dot(rows, up_w[...])).astype(BF16)
+        gate = dot(rows[...], gate_w[...])
+        return (gate / (1.0 + jnp.exp(-gate)) * dot(rows[...], up_w[...])).astype(BF16)
 
     act = jnp.concatenate([hidden(gate_own, up_own), hidden(gate_peer, up_peer)], axis=1)
     down = jnp.concatenate([down_own[...], down_peer[...]], axis=0)
-    outputs = dot(act, down)
-    for j in range(blocks):
-        wide[:, j, :] = outputs[:, j * LANES : (j + 1) * LANES]
-    out_ref[...] = wide[...].astype(BF16)
-
-
-def experts(rows, *weights):
+    outputs = dot(act, down).astype(BF16)
+    for first in range(0, count, 2 * blocks):
+        both = [stacked(outputs, first + i * blocks, blocks) for i in range(2)]
+        turned = dot(turn, jnp.concatenate(both, axis=1)).astype(BF16)
+        for i in range(2):
+            at = (first + i * blocks) * blocks
+            out_ref[at : at + size] = turned[:, i * LANES : (i + 1) * LANES]
+
+
+def experts(used, lines, *weights):
     vmem = pl.BlockSpec(memory_space=pltpu.VMEM)
     return pl.pallas_call(
         experts_kernel,
-        out_shape=pltpu.VMEM(rows.shape, BF16),
+        out_shape=pltpu.VMEM(lines.shape, BF16),
         in_specs=[vmem] * 7,
         out_specs=vmem,
-        scratch_shapes=[pltpu.VMEM(rows.shape, F32)],
-        compiler_params=pltpu.CompilerParams(vmem_limit_bytes=40 << 20),
+        scratch_shapes=[pltpu.VMEM((used, weights[0].shape[0]), BF16)],
+        compiler_params=pltpu.CompilerParams(vmem_limit_bytes=32 << 20),
         name="experts",
-    )(rows, *weights)
+    )(near(lines), *(near(w) for w in weights))
 
 
 def combine_kernel(
@@ -282,7 +342,8 @@
         total = jnp.zeros(wide.shape[1:], F32)
         for k in range(top):
             slot = slots[k, t]
-            row = returned_ref[jnp.maximum(slot, 0)].astype(F32)
+            at = pl.multiple_of(jnp.maximum(slot, 0) * wide.shape[1], wide.shape[1])
+            row = returned_ref[pl.ds(at, wide.shape[1]), :].astype(F32)
             total = total + jnp.where(slot >= 0, row * shares[k, t], 0.0)
         wide[t] = total
     half = wide.shape[1] // 2
@@ -313,11 +374,20 @@
             pltpu.SMEM(slots.shape, jnp.int32),
             pltpu.SemaphoreType.DMA((2,)),
         ],
+        compiler_params=pltpu.CompilerParams(vmem_limit_bytes=16 << 20),
         name="combine",
-    )(core, shares, slots, returned, resid)
-
-
-SLOTS_SPEC = pl.BlockSpec(memory_space=pl.ANY)
+    )(core, near(shares), near(slots), near(returned), near(resid))
+
+
+SLOTS_SPEC = pl.BlockSpec(memory_space=pltpu.VMEM)
+
+
+def near(array):
+    return pltpu.with_memory_space_constraint(array, pltpu.VMEM)
+
+
+def far(array):
+    return pltpu.with_memory_space_constraint(array, pltpu.HBM)
 
 
 def shards(
@@ -326,29 +396,30 @@
     expert_down,
 ):
     seqs, width = tokens.shape
-    places, head = key_cache.shape[1], key_cache.shape[3]
+    head = key_cache.shape[3]
     n_exp = expert_gate.shape[0] * lax.axis_size("ep")
     share = max(2, 2 * seqs * routes.shape[1] // n_exp) // 2
     used, blocks = n_exp * share, width // LANES
     swap = [(0, 1), (1, 0)]
     core = lax.axis_index("tp").reshape(1)
-    own, slots = attention(
+    stored = (expert_gate[0], expert_up[0], expert_down[0])
+    own, slots, *weights = attention(
         share, tokens, norm_gain.reshape(blocks, LANES), w_query, key_weight, value_weight,
-        forget_weight.T, w_out, key_cache.reshape(seqs, places, head),
-        cached_values.reshape(seqs, places, head), cum_gates.reshape(-1, LANES), lengths,
-        routes.T, core,
+        forget_weight.T, w_out, key_cache.reshape(-1, head),
+        cached_values.reshape(-1, head), cum_gates.reshape(-1, LANES), lengths,
+        routes.T, core, stored,
     )
     peer = lax.ppermute(own, "tp", swap)
-    weights = (expert_gate[0], expert_up[0], expert_down[0])
+    send, resid = dispatch(used, tokens, own, peer, expert_gain.reshape(blocks, LANES), slots)
+    *weights, send = lax.optimization_barrier((*weights, send))
     other = tuple(lax.ppermute(w, "tp", swap) for w in weights)
-    send, resid = dispatch(used, tokens, own, peer, expert_gain.reshape(blocks, LANES), slots)
-
-    def exchange(rows):
-        slabs = rows.reshape(n_exp, share * blocks, LANES)
+
+    def exchange(lines):
+        slabs = lines.reshape(n_exp, share * blocks, LANES)
         slabs = lax.all_to_all(slabs, "ep", split_axis=0, concat_axis=0, tiled=True)
-        return slabs.reshape(used, blocks, LANES)
-
-    outputs = experts(exchange(send), *weights, *other)
+        return slabs.reshape(used * blocks, LANES)
+
+    outputs = experts(used, exchange(send), *weights, *other)
     keep, give = combine(exchange(outputs), slots, route_weights.T, resid, core)
     got = lax.ppermute(give, "tp", swap)
     return (keep + got).astype(BF16)

time: 78.8 us -> 68.9 us (0.87)
  Pallas kernels: 22.8 us -> 15.6 us
  local copies, waits for them, and re-layouts: 1.91 us -> 0.01 us
  blocking collectives: 45.4 us -> 44.6 us
    pallas_call x3, Pallas kernels: 20.2 us -> 14.2 us  [the longest x1 11.2 us: attention(): pl.pallas_call(functools.partial(attention_kernel, share), out_shape=(plt...]
    unnamed x10 -> x6, local copies, waits for them, and re-layouts: 1.91 us -> 0.01 us
    ppermute x1, starting transfers between devices: 0.08 us -> 1.45 us  [shards(): peer = lax.ppermute(own, 'tp', swap)]
    pallas_call x1, Pallas kernels: 2.59 us -> 1.4 us  [combine(): pl.pallas_call(combine_kernel, out_shape=(half, half), in_specs=[pl.Block...]
    ppermute x3, starting transfers between devices: 1.89 us -> 0.96 us  [shards(): other = tuple((lax.ppermute(w, 'tp', swap) for w in weights))]
  transfers between devices with their start and end apart: 5 -> 5, of which waited for: 2 -> 2; matrix products, arithmetic and copies ran while one was open for 0% -> 0% of each run, Pallas kernels for 19% -> 0%
where the time goes in v3:
time: 68.9 us; the launch traced here: 68.7 us
  blocking collectives  44.6 us (65%)
  Pallas kernels  15.6 us (23%)
  starting transfers between devices  5.58 us (8%)
  waiting for transfers between devices  2.15 us (3%)
    all_to_all x2, blocking collectives, exchange(): slabs = lax.all_to_all(slabs, 'ep', split_axis=0, concat_axis=0, tiled=True)  44.6 us
    pallas_call x1, Pallas kernels, attention(): pl.pallas_call(functools.partial(attention_kernel, share), out_shape=(plt...  11.2 us
    ppermute x1, starting transfers between devices, shards(): got = lax.ppermute(give, 'tp', swap)  3.17 us
    pallas_call x1, Pallas kernels, experts(): pl.pallas_call(experts_kernel, out_shape=pltpu.VMEM(lines.shape, BF16), i...  2.02 us
    ppermute x1, starting transfers between devices, shards(): peer = lax.ppermute(own, 'tp', swap)  1.45 us
    pallas_call x1, Pallas kernels, combine(): pl.pallas_call(combine_kernel, out_shape=(half, half), in_specs=[pl.Block...  1.4 us
  transfers between devices with their start and end apart: 5, of which 2 were waited for; matrix products, arithmetic and copies ran while one was open for 0% of the time, Pallas kernels for 0%

profile of v3, /device:TPU:1, one launch (start us, length us, event | category | flops | bytes accessed | tf_op | source)
XLA Modules:
  0.0 68.7 jit_solution(17212267156100741072)
XLA Ops:
  0.0 0.0 copy-start
  0.0 0.0 copy-start.1
  0.0 0.0 copy-start.2
  0.0 11.2 %attention.1 = (bf16[48,2048]{1,0:T(8,128)(2,1)S(1)}, s32[4,48]{1,0:T(4,128)S(1)}, bf16[2048,256]{1,0:T(8,128)(2,1)S(1)}, bf16[2048,256]{1,0:T(8,128)(2,1)S(1)}, bf16[256,2048]{1,0:T(8,128)(2,1)S(1)}) custom-call(s32[48]{0:T(128)} %lengths.1, s32[1]{0:T(128)} %bitcast.core, bf16[48,2048]{1,0:T(8,128)(2,1)} %tokens_ref.1, bf16[16,128]{1,0:T(8,128)(2,1)} %bitcast.29, ...), custom_call_target="tpu_custom_call" | custom-call | tf_op jit(solution)/shard_map/attention/pallas_call | solution.py:200
  11.2 1.4 %collective-permute-start = (bf16[48,2048]{1,0:T(8,128)(2,1)S(1)}, bf16[48,2048]{1,0:T(8,128)(2,1)S(1)}, u32[]{:S(2)}, u32[]{:S(2)}) collective-permute-start(bf16[48,2048]{1,0:T(8,128)(2,1)S(1)} %get-tuple-element.22.own_ref), channel_id=1, source_target_pairs={{0,1},{1,0},{2,3},{3,2},{4,5},{5,4},{6,7},{7,6},{8,9},{9,8},{10,11... | collective-permute-start | bytes 589832 | tf_op jit(solution)/shard_map/ppermute | solution.py:412
  12.6 1.1 %collective-permute-done.peer_ref = bf16[48,2048]{1,0:T(8,128)(2,1)S(1)} collective-permute-done((bf16[48,2048]{1,0:T(8,128)(2,1)S(1)}, bf16[48,2048]{1,0:T(8,128)(2,1)S(1)}, u32[]{:S(2)}, u32[]{:S(2)}) %collective-permute-start) | collective-permute-done | bytes 196640 | tf_op jit(solution)/shard_map/ppermute | solution.py:412
  13.7 0.0 copy-done
  13.7 0.0 copy-done.1
  13.7 1.0 %dispatch.1 = (bf16[3072,128]{1,0:T(8,128)(2,1)S(1)}, bf16[48,2048]{1,0:T(8,128)(2,1)S(1)}) custom-call(bf16[48,2048]{1,0:T(8,128)(2,1)S(1)} %copy-done, bf16[48,2048]{1,0:T(8,128)(2,1)S(1)} %get-tuple-element.22.own_ref, bf16[48,2048]{1,0:T(8,128)(2,1)S(1)} %collective-permute-done.peer_ref, bf16[16,128]{1,0:T(8,128)(2,1)S(1)} %bitcast.20, ...), custom_call_target="tpu_custom_call" | custom-call | tf_op jit(solution)/shard_map/dispatch/pallas_call | solution.py:268
  14.7 0.5 collective-permute-start.1
  15.2 0.1 collective-permute-start.2
  15.3 0.4 collective-permute-start.3
  15.7 26.5 %all_to_all.10 = bf16[64,48,128]{2,1,0:T(8,128)(2,1)S(1)} all-to-all(bf16[64,48,128]{2,1,0:T(8,128)(2,1)S(1)} %bitcast.19), channel_id=1, replica_groups=mesh['ep'=64,'tp'=2] {'ep'}, dimensions={0} | all-to-all | bytes 1572864 | tf_op jit(solution)/shard_map/all_to_all | solution.py:419
  42.2 0.0 collective-permute-done.1.gate_peer
  42.2 0.0 collective-permute-done.2.up_peer
  42.2 0.0 collective-permute-done.3.down_peer
  42.2 2.0 %experts.1 = bf16[3072,128]{1,0:T(8,128)(2,1)S(1)} custom-call(bf16[3072,128]{1,0:T(8,128)(2,1)S(1)} %bitcast.17, bf16[2048,256]{1,0:T(8,128)(2,1)S(1)} %get-tuple-element.25.gate_own, bf16[2048,256]{1,0:T(8,128)(2,1)S(1)} %get-tuple-element.26.up_own, bf16[256,2048]{1,0:T(8,128)(2,1)S(1)} %get-tuple-element.27.down_own, ...), custom_call_target="tpu_custom_call" | custom-call | tf_op jit(solution)/shard_map/experts/pallas_call | solution.py:318
  44.2 18.1 %all_to_all.11 = bf16[64,48,128]{2,1,0:T(8,128)(2,1)S(1)} all-to-all(bf16[64,48,128]{2,1,0:T(8,128)(2,1)S(1)} %bitcast.18), channel_id=1, replica_groups=mesh['ep'=64,'tp'=2] {'ep'}, dimensions={0} | all-to-all | bytes 1572864 | tf_op jit(solution)/shard_map/all_to_all | solution.py:419
  62.3 0.0 copy-done.2
  62.4 1.4 %combine.1 = (f32[48,1024]{1,0:T(8,128)S(1)}, f32[48,1024]{1,0:T(8,128)S(1)}) custom-call(s32[1]{0:T(128)} %bitcast.core, f32[4,48]{1,0:T(4,128)S(1)} %bitcast.21, s32[4,48]{1,0:T(4,128)S(1)} %get-tuple-element.18.slots_any, bf16[3072,128]{1,0:T(8,128)(2,1)S(1)} %bitcast.16, bf16[48,2048]{1,0:T(8,128)(2,1)S(1)} %get-tuple-element.28.resid_ref), custom_call_target="tpu_custom_call" | custom-call | tf_op jit(solution)/shard_map/combine/pallas_call | solution.py:366
  63.8 3.2 %collective-permute-start.4 = (f32[48,1024]{1,0:T(8,128)S(1)}, f32[48,1024]{1,0:T(8,128)S(1)}, u32[]{:S(2)}, u32[]{:S(2)}) collective-permute-start(f32[48,1024]{1,0:T(8,128)S(1)} %get-tuple-element.30), channel_id=1, source_target_pairs={{0,1},{1,0},{2,3},{3,2},{4,5},{5,4},{6,7},{7,6},{8,9},{9,8},{10,11... | collective-permute-start | bytes 589832 | tf_op jit(solution)/shard_map/ppermute | solution.py:424
  66.9 1.1 %collective-permute-done.4 = f32[48,1024]{1,0:T(8,128)S(1)} collective-permute-done((f32[48,1024]{1,0:T(8,128)S(1)}, f32[48,1024]{1,0:T(8,128)S(1)}, u32[]{:S(2)}, u32[]{:S(2)}) %collective-permute-start.4) | collective-permute-done | bytes 196640 | tf_op jit(solution)/shard_map/ppermute | solution.py:424
  68.0 0.7 add_convert_fusion
Async XLA Ops:
  0.0 13.7 %copy-start = (bf16[48,2048]{1,0:T(8,128)(2,1)S(1)}, bf16[48,2048]{1,0:T(8,128)(2,1)}, u32[]{:S(2)}) copy-start(bf16[48,2048]{1,0:T(8,128)(2,1)} %tokens_ref.1) | copy-start | bytes 589828
  0.0 13.7 %copy-start.1 = (bf16[2048]{0:T(1024)(128)(2,1)S(1)}, bf16[2048]{0:T(1024)(128)(2,1)}, u32[]{:S(2)}) copy-start(bf16[2048]{0:T(1024)(128)(2,1)} %param.19) | copy-start | bytes 12292
  0.0 62.3 %copy-start.2 = (f32[48,4]{0,1:T(4,128)S(1)}, f32[48,4]{0,1:T(4,128)}, u32[]{:S(2)}) copy-start(f32[48,4]{0,1:T(4,128)} %param.30) | copy-start | bytes 2308
  11.2 2.5 %collective-permute-start = (bf16[48,2048]{1,0:T(8,128)(2,1)S(1)}, bf16[48,2048]{1,0:T(8,128)(2,1)S(1)}, u32[]{:S(2)}, u32[]{:S(2)}) collective-permute-start(bf16[48,2048]{1,0:T(8,128)(2,1)S(1)} %get-tuple-element.22.own_ref), channel_id=1, source_target_pairs={{0,1},{1,0},{2,3},{3,2},{4,5},{5,4},{6,7},{7,6},{8,9},{9,8},{10,11... | collective-permute-start | bytes 589832 | tf_op jit(solution)/shard_map/ppermute | solution.py:412
  14.7 27.5 %collective-permute-start.1 = (bf16[2048,256]{1,0:T(8,128)(2,1)S(1)}, bf16[2048,256]{1,0:T(8,128)(2,1)S(1)}, u32[]{:S(2)}, u32[]{:S(2)}) collective-permute-start(bf16[2048,256]{1,0:T(8,128)(2,1)S(1)} %get-tuple-element.25.gate_own), channel_id=1, source_target_pairs={{0,1},{1,0},{2,3},{3,2},{4,5},{5,4},{6,7},{7,6},{8,9},{9,8},{10,11... | collective-permute-start | bytes 3145736 | tf_op jit(solution)/shard_map/ppermute | solution.py:415
  15.2 27.0 %collective-permute-start.2 = (bf16[2048,256]{1,0:T(8,128)(2,1)S(1)}, bf16[2048,256]{1,0:T(8,128)(2,1)S(1)}, u32[]{:S(2)}, u32[]{:S(2)}) collective-permute-start(bf16[2048,256]{1,0:T(8,128)(2,1)S(1)} %get-tuple-element.26.up_own), channel_id=1, source_target_pairs={{0,1},{1,0},{2,3},{3,2},{4,5},{5,4},{6,7},{7,6},{8,9},{9,8},{10,11... | collective-permute-start | bytes 3145736 | tf_op jit(solution)/shard_map/ppermute | solution.py:415
  15.3 26.9 %collective-permute-start.3 = (bf16[256,2048]{1,0:T(8,128)(2,1)S(1)}, bf16[256,2048]{1,0:T(8,128)(2,1)S(1)}, u32[]{:S(2)}, u32[]{:S(2)}) collective-permute-start(bf16[256,2048]{1,0:T(8,128)(2,1)S(1)} %get-tuple-element.27.down_own), channel_id=1, source_target_pairs={{0,1},{1,0},{2,3},{3,2},{4,5},{5,4},{6,7},{7,6},{8,9},{9,8},{10,11... | collective-permute-start | bytes 3145736 | tf_op jit(solution)/shard_map/ppermute | solution.py:415
  63.8 4.2 %collective-permute-start.4 = (f32[48,1024]{1,0:T(8,128)S(1)}, f32[48,1024]{1,0:T(8,128)S(1)}, u32[]{:S(2)}, u32[]{:S(2)}) collective-permute-start(f32[48,1024]{1,0:T(8,128)S(1)} %get-tuple-element.30), channel_id=1, source_target_pairs={{0,1},{1,0},{2,3},{3,2},{4,5},{5,4},{6,7},{7,6},{8,9},{9,8},{10,11... | collective-permute-start | bytes 589832 | tf_op jit(solution)/shard_map/ppermute | solution.py:424

commit v4 on v3

--- a/solution.py
+++ b/solution.py
@@ -32,17 +32,17 @@
 
 
 def attention_kernel(
-    share, lengths, core, tokens_hbm, gain_hbm, wq_hbm, wk_hbm, wv_hbm, forget_hbm, wo_hbm,
-    keys_hbm, values_hbm, gates_hbm, routes_hbm, gate_hbm, up_hbm, down_hbm, partial_ref, slots_ref,
-    gate_ref, up_ref, down_ref,
+    share, n_exp, lengths, core, tokens_hbm, gain_hbm, wq_hbm, wk_hbm, wv_hbm, forget_hbm, wo_hbm,
+    keys_hbm, values_hbm, gates_hbm, routes_hbm, gate_hbm, up_hbm, down_hbm, shares_hbm, partial_ref, places_ref,
+    parts_ref, pack_ref,
     tokens, gain, wq, wk, wv, forget, wo, keys, values, gates, routes, attended,
-    small_sems, key_sems, value_sems, weight_sems,
+    shares_ref, small_sems, key_sems, value_sems, weight_sems,
 ):
     seqs = attended.shape[0]
     places, head = keys.shape[0] // seqs, keys.shape[1]
     small = [
         (tokens_hbm, tokens), (gain_hbm, gain), (wq_hbm, wq), (wk_hbm, wk), (wv_hbm, wv),
-        (forget_hbm, forget), (gates_hbm, gates), (routes_hbm, routes), (wo_hbm, wo),
+        (forget_hbm, forget), (gates_hbm, gates), (routes_hbm, routes), (shares_hbm, shares_ref), (wo_hbm, wo),
     ]
     copies = [pltpu.make_async_copy(a, b, small_sems.at[i]) for i, (a, b) in enumerate(small)]
 
@@ -74,16 +74,13 @@
         c.start()
     spans = SPANS + ((), (), ())
     start(keys_hbm, keys, key_sems, spans[0])
-    for c in copies[:-1]:
+    for c in copies[:2]:
         c.wait()
-    start(keys_hbm, keys, key_sems, spans[1])
-    start_values(spans[0])
-    start(keys_hbm, keys, key_sems, spans[2])
-    start_values(spans[1])
-    copies[-1].start()
-
+    normed = scaled_rows(tokens[...].astype(F32), gain[...].astype(F32))
+    for c in copies[7:9]:
+        c.wait()
     named = routes[...]
-    top, n_exp = named.shape[0], 64
+    top, blocks = named.shape[0], gain.shape[0]
     expert = lax.broadcasted_iota(jnp.int32, (n_exp, seqs), 0)
     hits = [expert == named[k : k + 1, :] for k in range(top)]
     onehot = sum(h.astype(F32) for h in hits)
@@ -95,9 +92,15 @@
         rank = jnp.sum(jnp.where(hits[k], count, 0.0), axis=0, keepdims=True).astype(jnp.int32)
         rank = rank - core[0] * share
         mine = (rank >= 0) & (rank < share)
-        slots_ref[k : k + 1, :] = jnp.where(mine, named[k : k + 1, :] * share + rank, -1)
-
-    normed = scaled_rows(tokens[...].astype(F32), gain[...].astype(F32))
+        place = (named[k : k + 1, :] * share + rank) * blocks
+        places_ref[k : k + 1, :] = jnp.where(mine, place, n_exp * share * blocks)
+        places_ref[top + k : top + k + 1, :] = jnp.where(mine, place, 0)
+        parts_ref[k : k + 1, :] = jnp.where(mine, shares_ref[k : k + 1, :], 0.0)
+
+    start(keys_hbm, keys, key_sems, spans[1])
+    start_values(spans[0])
+    for c in copies[2:6]:
+        c.wait()
     query = dot(normed, wq[...]).astype(BF16)
     key_new = dot(normed, wk[...]).astype(BF16).astype(F32)
     value_new = dot(normed, wv[...]).astype(BF16).astype(F32)
@@ -106,6 +109,10 @@
     raw = jnp.sum(jnp.where(column, raw, 0.0), axis=1, keepdims=True)
     log_forget = jnp.minimum(raw, 0.0) - jnp.log1p(jnp.exp(-jnp.abs(raw)))
 
+    start(keys_hbm, keys, key_sems, spans[2])
+    start_values(spans[1])
+    copies[-1].start()
+    copies[6].wait()
     scale = head ** (-0.5)
     rows2 = lax.broadcasted_iota(jnp.int32, (2 * GROUP, 1), 0) % GROUP
     rows1 = lax.broadcasted_iota(jnp.int32, (GROUP, 1), 0)
@@ -167,7 +174,11 @@
         attended[own_rows, head:] = result[GROUP:]
 
     wait(keys_hbm, keys, key_sems, spans[0])
-    pairs = [(gate_hbm, gate_ref), (up_hbm, up_ref), (down_hbm, down_ref)]
+    width, inner = gate_hbm.shape
+    pairs = [(gate_hbm, pack_ref.at[:width]), (up_hbm, pack_ref.at[width : 2 * width])]
+    for first in range(0, width, inner):
+        at = 2 * width + first
+        pairs.append((down_hbm.at[:, first : first + inner], pack_ref.at[at : at + inner]))
     moved = [pltpu.make_async_copy(a, b, weight_sems.at[i]) for i, (a, b) in enumerate(pairs)]
     pending = [scores_of(g) for g in spans[0]]
     for i, span in enumerate(SPANS):
@@ -189,7 +200,8 @@
 
 
 def attention(
-    share, tokens, gain, wq, wk, wv, forget, wo, keys, values, gates, lengths, routes, core, weights
+    share, n_exp, tokens, gain, wq, wk, wv, forget, wo, keys, values, gates, lengths, routes, core,
+    weights, shares,
 ):
     seqs = tokens.shape[0]
     anywhere = pl.BlockSpec(memory_space=pl.ANY)
@@ -198,25 +210,29 @@
     inputs = (tokens, gain, wq, wk, wv, forget, wo, keys, values, gates, routes)
     order = (tokens, gain, wq, wk, wv, forget, wo, keys, values, gates, routes)
     return pl.pallas_call(
-        functools.partial(attention_kernel, share),
+        functools.partial(attention_kernel, share, n_exp),
         out_shape=(
             pltpu.VMEM(tokens.shape, BF16),
-            pltpu.VMEM(routes.shape, jnp.int32),
-            *(pltpu.VMEM(w.shape, w.dtype) for w in weights),
+            pltpu.VMEM((2 * routes.shape[0], routes.shape[1]), jnp.int32),
+            pltpu.VMEM(routes.shape, F32),
+            pltpu.VMEM((3 * weights[0].shape[0], weights[0].shape[1]), BF16),
         ),
-        in_specs=[scalar, scalar] + [anywhere] * len(inputs) + [hbm] * len(weights),
-        out_specs=[pl.BlockSpec(memory_space=pltpu.VMEM)] * (2 + len(weights)),
+        in_specs=[scalar, scalar] + [anywhere] * len(inputs)
+        + [hbm] * len(weights)
+        + [anywhere],
+        out_specs=[pl.BlockSpec(memory_space=pltpu.VMEM)] * 4,
         scratch_shapes=[pltpu.VMEM(a.shape, a.dtype) for a in order]
         + [
             pltpu.VMEM((seqs, wo.shape[0]), BF16),
-            pltpu.SemaphoreType.DMA((9,)),
+            pltpu.VMEM(shares.shape, F32),
+            pltpu.SemaphoreType.DMA((10,)),
             pltpu.SemaphoreType.DMA((seqs // GROUP,)),
             pltpu.SemaphoreType.DMA((seqs // GROUP,)),
-            pltpu.SemaphoreType.DMA((len(weights),)),
+            pltpu.SemaphoreType.DMA((2 + weights[0].shape[0] // weights[0].shape[1],)),
         ],
         compiler_params=pltpu.CompilerParams(vmem_limit_bytes=52 << 20),
         name="attention",
-    )(lengths, core, *inputs, *(far(w) for w in weights))
+    )(lengths, core, *inputs, *(far(w) for w in weights), shares)
 
 
 def swapped(blocks):
@@ -235,7 +251,7 @@
 def dispatch_kernel(
     tokens_ref, own_ref, peer_ref, gain_ref, slots_any, send_ref, resid_ref, lines, slots, sem
 ):
-    top, seqs = slots.shape
+    top, seqs = slots.shape[0] // 2, slots.shape[1]
     copy = pltpu.make_async_copy(slots_any, slots, sem)
     copy.start()
     blocks = gain_ref.shape[0]
@@ -255,9 +271,7 @@
         start = t % blocks * blocks
         row = by_token[t // blocks][start : start + blocks]
         for k in range(top):
-            slot = slots[k, t]
-            place = jnp.where(slot < 0, used, slot * blocks)
-            lines[pl.ds(pl.multiple_of(place, blocks), blocks), :] = row
+            lines[pl.ds(pl.multiple_of(slots[k, t], blocks), blocks), :] = row
     send_ref[...] = lines[:used]
 
 
@@ -280,9 +294,7 @@
     )(near(tokens), near(own), near(peer), near(gain), near(slots))
 
 
-def experts_kernel(
-    lines_ref, gate_own, up_own, down_own, gate_peer, up_peer, down_peer, out_ref, rows
-):
+def experts_kernel(lines_ref, own_ref, peer_ref, out_ref, rows):
     count, width = rows.shape
     blocks = width // LANES
     size = blocks * blocks
@@ -298,13 +310,19 @@
                     j * blocks : (j + 1) * blocks, i * LANES : (i + 1) * LANES
                 ]
 
-    def hidden(gate_w, up_w):
-        gate = dot(rows[...], gate_w[...])
-        return (gate / (1.0 + jnp.exp(-gate)) * dot(rows[...], up_w[...])).astype(BF16)
-
-    act = jnp.concatenate([hidden(gate_own, up_own), hidden(gate_peer, up_peer)], axis=1)
-    down = jnp.concatenate([down_own[...], down_peer[...]], axis=0)
-    outputs = dot(act, down).astype(BF16)
+    inner = own_ref.shape[1]
+
+    def hidden(pack):
+        gate = dot(rows[...], pack[:width])
+        upper = dot(rows[...], pack[width : 2 * width])
+        return (gate / (1.0 + jnp.exp(-gate)) * upper).astype(BF16)
+
+    act = jnp.concatenate([hidden(own_ref), hidden(peer_ref)], axis=1)
+    outputs = []
+    for first in range(2 * width, 3 * width, inner):
+        down = [pack[first : first + inner] for pack in (own_ref, peer_ref)]
+        outputs.append(dot(act, jnp.concatenate(down, axis=0)).astype(BF16))
+    outputs = jnp.concatenate(outputs, axis=1)
     for first in range(0, count, 2 * blocks):
         both = [stacked(outputs, first + i * blocks, blocks) for i in range(2)]
         turned = dot(turn, jnp.concatenate(both, axis=1)).astype(BF16)
@@ -313,70 +331,66 @@
             out_ref[at : at + size] = turned[:, i * LANES : (i + 1) * LANES]
 
 
-def experts(used, lines, *weights):
+def experts(used, lines, own, peer):
     vmem = pl.BlockSpec(memory_space=pltpu.VMEM)
     return pl.pallas_call(
         experts_kernel,
         out_shape=pltpu.VMEM(lines.shape, BF16),
-        in_specs=[vmem] * 7,
+        in_specs=[vmem] * 3,
         out_specs=vmem,
-        scratch_shapes=[pltpu.VMEM((used, weights[0].shape[0]), BF16)],
+        scratch_shapes=[pltpu.VMEM((used, own.shape[0] // 3), BF16)],
         compiler_params=pltpu.CompilerParams(vmem_limit_bytes=32 << 20),
         name="experts",
-    )(near(lines), *(near(w) for w in weights))
+    )(near(lines), near(own), near(peer))
 
 
 def combine_kernel(
-    core, shares_any, slots_any, returned_ref, resid_ref, keep_ref, give_ref, wide, shares, slots, sems
+    kept, core, shares_any, slots_any, returned_ref, *refs
 ):
-    top, seqs = slots.shape
+    *resid_refs, out_ref, wide, shares, slots, sems = refs
+    top, seqs = shares.shape
     copies = [
         pltpu.make_async_copy(slots_any, slots, sems.at[0]),
         pltpu.make_async_copy(shares_any, shares, sems.at[1]),
     ]
     for c in copies:
         c.start()
+    half = wide.shape[1]
+    which = core[0] if kept else 1 - core[0]
+    first = which * half
     for c in copies:
         c.wait()
     for t in range(seqs):
         total = jnp.zeros(wide.shape[1:], F32)
         for k in range(top):
-            slot = slots[k, t]
-            at = pl.multiple_of(jnp.maximum(slot, 0) * wide.shape[1], wide.shape[1])
-            row = returned_ref[pl.ds(at, wide.shape[1]), :].astype(F32)
-            total = total + jnp.where(slot >= 0, row * shares[k, t], 0.0)
+            at = pl.multiple_of(slots[top + k, t] + first, half)
+            total = total + returned_ref[pl.ds(at, half), :].astype(F32) * shares[k, t]
         wide[t] = total
-    half = wide.shape[1] // 2
-    width = half * LANES
-    mine = core[0]
-
-    def columns(which):
-        return jnp.concatenate([wide[:, which * half + j, :] for j in range(half)], axis=1)
-
-    resid = jnp.where(mine == 0, resid_ref[:, :width], resid_ref[:, width:])
-    keep_ref[...] = columns(mine) + resid.astype(F32)
-    give_ref[...] = columns(1 - mine)
-
-
-def combine(returned, slots, shares, resid, core):
-    seqs, width = resid.shape
-    blocks = width // LANES
+    columns = jnp.concatenate([wide[:, j, :] for j in range(half)], axis=1)
+    for ref in resid_refs:
+        width = half * LANES
+        resid = jnp.where(which == 0, ref[:, :width], ref[:, width:])
+        columns = columns + resid.astype(F32)
+    out_ref[...] = columns
+
+
+def combine(half, kept, returned, slots, shares, core, *resid):
+    seqs = slots.shape[1]
     vmem = pl.BlockSpec(memory_space=pltpu.VMEM)
-    half = pltpu.VMEM((seqs, width // 2), F32)
     return pl.pallas_call(
-        combine_kernel,
-        out_shape=(half, half),
-        in_specs=[pl.BlockSpec(memory_space=pltpu.SMEM), SLOTS_SPEC, SLOTS_SPEC, vmem, vmem],
-        out_specs=(vmem, vmem),
+        functools.partial(combine_kernel, kept),
+        out_shape=pltpu.VMEM((seqs, half * LANES), F32),
+        in_specs=[pl.BlockSpec(memory_space=pltpu.SMEM)] + [vmem] * (3 + len(resid)),
+        out_specs=vmem,
         scratch_shapes=[
-            pltpu.VMEM((seqs, blocks, LANES), F32),
+            pltpu.VMEM((seqs, half, LANES), F32),
             pltpu.SMEM(shares.shape, F32),
             pltpu.SMEM(slots.shape, jnp.int32),
             pltpu.SemaphoreType.DMA((2,)),
         ],
         compiler_params=pltpu.CompilerParams(vmem_limit_bytes=16 << 20),
-        name="combine",
-    )(core, near(shares), near(slots), near(returned), near(resid))
+        name="keep" if kept else "give",
+    )(core, near(shares), near(slots), near(returned), *(near(r) for r in resid))
 
 
 SLOTS_SPEC = pl.BlockSpec(memory_space=pltpu.VMEM)
@@ -403,25 +417,27 @@
     swap = [(0, 1), (1, 0)]
     core = lax.axis_index("tp").reshape(1)
     stored = (expert_gate[0], expert_up[0], expert_down[0])
-    own, slots, *weights = attention(
-        share, tokens, norm_gain.reshape(blocks, LANES), w_query, key_weight, value_weight,
+    own, slots, parts, pack = attention(
+        share, n_exp, tokens, norm_gain.reshape(blocks, LANES), w_query, key_weight, value_weight,
         forget_weight.T, w_out, key_cache.reshape(-1, head),
         cached_values.reshape(-1, head), cum_gates.reshape(-1, LANES), lengths,
-        routes.T, core, stored,
+        routes.T, core, stored, route_weights.T,
     )
     peer = lax.ppermute(own, "tp", swap)
     send, resid = dispatch(used, tokens, own, peer, expert_gain.reshape(blocks, LANES), slots)
-    *weights, send = lax.optimization_barrier((*weights, send))
-    other = tuple(lax.ppermute(w, "tp", swap) for w in weights)
+    pack, send = lax.optimization_barrier((pack, send))
+    other = lax.ppermute(pack, "tp", swap)
 
     def exchange(lines):
         slabs = lines.reshape(n_exp, share * blocks, LANES)
         slabs = lax.all_to_all(slabs, "ep", split_axis=0, concat_axis=0, tiled=True)
         return slabs.reshape(used * blocks, LANES)
 
-    outputs = experts(used, exchange(send), *weights, *other)
-    keep, give = combine(exchange(outputs), slots, route_weights.T, resid, core)
+    outputs = experts(used, exchange(send), pack, other)
+    returned = exchange(outputs)
+    give = combine(blocks // 2, False, returned, slots, parts, core)
     got = lax.ppermute(give, "tp", swap)
+    keep = combine(blocks // 2, True, returned, slots, parts, core, resid)
     return (keep + got).astype(BF16)
 
 

time: 68.9 us -> 67.6 us (0.981)
  waiting for transfers between devices: 2.15 us -> 1.08 us
    ppermute x1, waiting for transfers between devices: 1.07 us -> 0.01 us  [shards(): got = lax.ppermute(give, 'tp', swap)]
    pallas_call x2 -> x3, Pallas kernels: 12.6 us -> 12.8 us  [the longest x1 10.7 us: attention(): pl.pallas_call(functools.partial(attention_kernel, share, n_exp), out_sha...]
  transfers between devices with their start and end apart: 5 -> 3, of which waited for: 2 -> 1; matrix products, arithmetic and copies ran while one was open for 0% -> 0% of each run, Pallas kernels for 0% -> 2%
where the time goes in v4:
time: 67.6 us; the launch traced here: 67.5 us
  blocking collectives  44.9 us (66%)
  Pallas kernels  15.7 us (23%)
  starting transfers between devices  5.09 us (8%)
  waiting for transfers between devices  1.08 us (2%)
    all_to_all x2, blocking collectives, exchange(): slabs = lax.all_to_all(slabs, 'ep', split_axis=0, concat_axis=0, tiled=True)  44.9 us
    pallas_call x1, Pallas kernels, attention(): pl.pallas_call(functools.partial(attention_kernel, share, n_exp), out_sha...  10.7 us
    ppermute x1, starting transfers between devices, shards(): got = lax.ppermute(give, 'tp', swap)  3.18 us
    pallas_call x2, Pallas kernels, combine(): pl.pallas_call(functools.partial(combine_kernel, kept), out_shape=pltpu.V...  2.12 us
    pallas_call x1, Pallas kernels, experts(): pl.pallas_call(experts_kernel, out_shape=pltpu.VMEM(lines.shape, BF16), i...  2.04 us
    ppermute x1, starting transfers between devices, shards(): peer = lax.ppermute(own, 'tp', swap)  1.46 us
  transfers between devices with their start and end apart: 3, of which 1 were waited for; matrix products, arithmetic and copies ran while one was open for 0% of the time, Pallas kernels for 2%

profile of v4, /device:TPU:1, one launch (start us, length us, event | category | flops | bytes accessed | tf_op | source)
XLA Modules:
  0.0 67.5 jit_solution(17398030446038557084)
XLA Ops:
  0.0 0.0 copy-start
  0.0 0.0 copy-start.1
  0.0 10.7 %attention.1 = (bf16[48,2048]{1,0:T(8,128)(2,1)S(1)}, s32[8,48]{1,0:T(8,128)S(1)}, f32[4,48]{1,0:T(4,128)S(1)}, bf16[6144,256]{1,0:T(8,128)(2,1)S(1)}) custom-call(s32[48]{0:T(128)} %lengths.1, s32[1]{0:T(128)} %bitcast.core, bf16[48,2048]{1,0:T(8,128)(2,1)} %tokens_ref.1, bf16[16,128]{1,0:T(8,128)(2,1)} %bitcast.29, bf16[2048,256]{1,0:T(8,128)(2,1)} %wq_hbm.1, ...), custom_call_target="tpu_custom_call" | custom-call | tf_op jit(solution)/shard_map/attention/pallas_call | solution.py:212
  10.7 1.5 %collective-permute-start = (bf16[48,2048]{1,0:T(8,128)(2,1)S(1)}, bf16[48,2048]{1,0:T(8,128)(2,1)S(1)}, u32[]{:S(2)}, u32[]{:S(2)}) collective-permute-start(bf16[48,2048]{1,0:T(8,128)(2,1)S(1)} %get-tuple-element.16.own_ref), channel_id=1, source_target_pairs={{0,1},{1,0},{2,3},{3,2},{4,5},{5,4},{6,7},{7,6},{8,9},{9,8},{10,11... | collective-permute-start | bytes 589832 | tf_op jit(solution)/shard_map/ppermute | solution.py:426
  12.2 1.1 %collective-permute-done.peer_ref = bf16[48,2048]{1,0:T(8,128)(2,1)S(1)} collective-permute-done((bf16[48,2048]{1,0:T(8,128)(2,1)S(1)}, bf16[48,2048]{1,0:T(8,128)(2,1)S(1)}, u32[]{:S(2)}, u32[]{:S(2)}) %collective-permute-start) | collective-permute-done | bytes 196640 | tf_op jit(solution)/shard_map/ppermute | solution.py:426
  13.2 0.0 copy-done
  13.2 0.0 copy-done.1
  13.3 0.9 %dispatch.1 = (bf16[3072,128]{1,0:T(8,128)(2,1)S(1)}, bf16[48,2048]{1,0:T(8,128)(2,1)S(1)}) custom-call(bf16[48,2048]{1,0:T(8,128)(2,1)S(1)} %copy-done, bf16[48,2048]{1,0:T(8,128)(2,1)S(1)} %get-tuple-element.16.own_ref, bf16[48,2048]{1,0:T(8,128)(2,1)S(1)} %collective-permute-done.peer_ref, bf16[16,128]{1,0:T(8,128)(2,1)S(1)} %bitcast.21, ...), custom_call_target="tpu_custom_call" | custom-call | tf_op jit(solution)/shard_map/dispatch/pallas_call | solution.py:282
  14.1 0.5 collective-permute-start.1
  14.6 26.8 %all_to_all.10 = bf16[64,48,128]{2,1,0:T(8,128)(2,1)S(1)} all-to-all(bf16[64,48,128]{2,1,0:T(8,128)(2,1)S(1)} %bitcast.20), channel_id=1, replica_groups=mesh['ep'=64,'tp'=2] {'ep'}, dimensions={0} | all-to-all | bytes 1572864 | tf_op jit(solution)/shard_map/all_to_all | solution.py:433
  41.4 0.0 collective-permute-done.1.peer_ref
  41.4 2.0 %experts.1 = bf16[3072,128]{1,0:T(8,128)(2,1)S(1)} custom-call(bf16[3072,128]{1,0:T(8,128)(2,1)S(1)} %bitcast.18, bf16[6144,256]{1,0:T(8,128)(2,1)S(1)} %get-tuple-element.19.own_ref, bf16[6144,256]{1,0:T(8,128)(2,1)S(1)} %collective-permute-done.1.peer_ref), custom_call_target="tpu_custom_call" | custom-call | tf_op jit(solution)/shard_map/experts/pallas_call | solution.py:336
  43.4 18.1 %all_to_all.11 = bf16[64,48,128]{2,1,0:T(8,128)(2,1)S(1)} all-to-all(bf16[64,48,128]{2,1,0:T(8,128)(2,1)S(1)} %bitcast.19), channel_id=1, replica_groups=mesh['ep'=64,'tp'=2] {'ep'}, dimensions={0} | all-to-all | bytes 1572864 | tf_op jit(solution)/shard_map/all_to_all | solution.py:433
  61.5 1.0 %give.1 = f32[48,1024]{1,0:T(8,128)S(1)} custom-call(s32[1]{0:T(128)} %bitcast.core, f32[4,48]{1,0:T(4,128)S(1)} %get-tuple-element.13.shares_any, s32[8,48]{1,0:T(8,128)S(1)} %get-tuple-element.14.slots_any, bf16[3072,128]{1,0:T(8,128)(2,1)S(1)} %bitcast.16), custom_call_target="tpu_custom_call" | custom-call | tf_op jit(solution)/shard_map/give/pallas_call | solution.py:380
  62.6 3.2 %collective-permute-start.2 = (f32[48,1024]{1,0:T(8,128)S(1)}, f32[48,1024]{1,0:T(8,128)S(1)}, u32[]{:S(2)}, u32[]{:S(2)}) collective-permute-start(f32[48,1024]{1,0:T(8,128)S(1)} %give.1), channel_id=1, source_target_pairs={{0,1},{1,0},{2,3},{3,2},{4,5},{5,4},{6,7},{7,6},{8,9},{9,8},{10,11... | collective-permute-start | bytes 589832 | tf_op jit(solution)/shard_map/ppermute | solution.py:439
  65.8 1.1 %keep.1 = f32[48,1024]{1,0:T(8,128)S(1)} custom-call(s32[1]{0:T(128)} %bitcast.core, f32[4,48]{1,0:T(4,128)S(1)} %get-tuple-element.13.shares_any, s32[8,48]{1,0:T(8,128)S(1)} %get-tuple-element.14.slots_any, bf16[3072,128]{1,0:T(8,128)(2,1)S(1)} %bitcast.17, bf16[48,2048]{1,0:T(8,128)(2,1)S(1)} %get-tuple-element.20.refs_0_), custom_call_target="tpu_custom_call" | custom-call | tf_op jit(solution)/shard_map/keep/pallas_call | solution.py:380
  66.8 0.0 collective-permute-done.2
  66.8 0.7 add_convert_fusion
Async XLA Ops:
  0.0 13.2 %copy-start = (bf16[48,2048]{1,0:T(8,128)(2,1)S(1)}, bf16[48,2048]{1,0:T(8,128)(2,1)}, u32[]{:S(2)}) copy-start(bf16[48,2048]{1,0:T(8,128)(2,1)} %tokens_ref.1) | copy-start | bytes 589828
  0.0 13.2 %copy-start.1 = (bf16[2048]{0:T(1024)(128)(2,1)S(1)}, bf16[2048]{0:T(1024)(128)(2,1)}, u32[]{:S(2)}) copy-start(bf16[2048]{0:T(1024)(128)(2,1)} %param.19) | copy-start | bytes 12292
  10.7 2.5 %collective-permute-start = (bf16[48,2048]{1,0:T(8,128)(2,1)S(1)}, bf16[48,2048]{1,0:T(8,128)(2,1)S(1)}, u32[]{:S(2)}, u32[]{:S(2)}) collective-permute-start(bf16[48,2048]{1,0:T(8,128)(2,1)S(1)} %get-tuple-element.16.own_ref), channel_id=1, source_target_pairs={{0,1},{1,0},{2,3},{3,2},{4,5},{5,4},{6,7},{7,6},{8,9},{9,8},{10,11... | collective-permute-start | bytes 589832 | tf_op jit(solution)/shard_map/ppermute | solution.py:426
  14.1 27.3 %collective-permute-start.1 = (bf16[6144,256]{1,0:T(8,128)(2,1)S(1)}, bf16[6144,256]{1,0:T(8,128)(2,1)S(1)}, u32[]{:S(2)}, u32[]{:S(2)}) collective-permute-start(bf16[6144,256]{1,0:T(8,128)(2,1)S(1)} %get-tuple-element.19.own_ref), channel_id=1, source_target_pairs={{0,1},{1,0},{2,3},{3,2},{4,5},{5,4},{6,7},{7,6},{8,9},{9,8},{10,11... | collective-permute-start | bytes 9437192 | tf_op jit(solution)/shard_map/ppermute | solution.py:429
  62.6 4.3 %collective-permute-start.2 = (f32[48,1024]{1,0:T(8,128)S(1)}, f32[48,1024]{1,0:T(8,128)S(1)}, u32[]{:S(2)}, u32[]{:S(2)}) collective-permute-start(f32[48,1024]{1,0:T(8,128)S(1)} %give.1), channel_id=1, source_target_pairs={{0,1},{1,0},{2,3},{3,2},{4,5},{5,4},{6,7},{7,6},{8,9},{9,8},{10,11... | collective-permute-start | bytes 589832 | tf_op jit(solution)/shard_map/ppermute | solution.py:439

commit v5 on v4

--- a/solution.py
+++ b/solution.py
@@ -371,7 +371,7 @@
         width = half * LANES
         resid = jnp.where(which == 0, ref[:, :width], ref[:, width:])
         columns = columns + resid.astype(F32)
-    out_ref[...] = columns
+    out_ref[...] = columns.astype(out_ref.dtype)
 
 
 def combine(half, kept, returned, slots, shares, core, *resid):
@@ -379,7 +379,7 @@
     vmem = pl.BlockSpec(memory_space=pltpu.VMEM)
     return pl.pallas_call(
         functools.partial(combine_kernel, kept),
-        out_shape=pltpu.VMEM((seqs, half * LANES), F32),
+        out_shape=pltpu.VMEM((seqs, half * LANES), F32 if kept else BF16),
         in_specs=[pl.BlockSpec(memory_space=pltpu.SMEM)] + [vmem] * (3 + len(resid)),
         out_specs=vmem,
         scratch_shapes=[
@@ -438,7 +438,7 @@
     give = combine(blocks // 2, False, returned, slots, parts, core)
     got = lax.ppermute(give, "tp", swap)
     keep = combine(blocks // 2, True, returned, slots, parts, core, resid)
-    return (keep + got).astype(BF16)
+    return (keep + got.astype(F32)).astype(BF16)
 
 
 def solution(mesh):

time: 67.6 us -> 67.5 us (level)
  no operation moved by 1% of the time
where the time goes in v5:
time: 67.5 us; the launch traced here: 67.3 us
  blocking collectives  44.6 us (66%)
  Pallas kernels  15.8 us (23%)
  starting transfers between devices  5.08 us (8%)
  waiting for transfers between devices  1.08 us (2%)
    all_to_all x2, blocking collectives, exchange(): slabs = lax.all_to_all(slabs, 'ep', split_axis=0, concat_axis=0, tiled=True)  44.6 us
    pallas_call x1, Pallas kernels, attention(): pl.pallas_call(functools.partial(attention_kernel, share, n_exp), out_sha...  10.7 us
    ppermute x1, starting transfers between devices, shards(): got = lax.ppermute(give, 'tp', swap)  3.17 us
    pallas_call x2, Pallas kernels, combine(): pl.pallas_call(functools.partial(combine_kernel, kept), out_shape=pltpu.V...  2.12 us
    pallas_call x1, Pallas kernels, experts(): pl.pallas_call(experts_kernel, out_shape=pltpu.VMEM(lines.shape, BF16), i...  2.03 us
    ppermute x1, starting transfers between devices, shards(): peer = lax.ppermute(own, 'tp', swap)  1.46 us
  transfers between devices with their start and end apart: 3, of which 1 were waited for; matrix products, arithmetic and copies ran while one was open for 0% of the time, Pallas kernels for 2%

profile of v5, /device:TPU:1, one launch (start us, length us, event | category | flops | bytes accessed | tf_op | source)
XLA Modules:
  0.0 67.3 jit_solution(17281440407756679879)
XLA Ops:
  0.0 0.0 copy-start
  0.0 0.0 copy-start.1
  0.0 10.7 %attention.1 = (bf16[48,2048]{1,0:T(8,128)(2,1)S(1)}, s32[8,48]{1,0:T(8,128)S(1)}, f32[4,48]{1,0:T(4,128)S(1)}, bf16[6144,256]{1,0:T(8,128)(2,1)S(1)}) custom-call(s32[48]{0:T(128)} %lengths.1, s32[1]{0:T(128)} %bitcast.core, bf16[48,2048]{1,0:T(8,128)(2,1)} %tokens_ref.1, bf16[16,128]{1,0:T(8,128)(2,1)} %bitcast.29, bf16[2048,256]{1,0:T(8,128)(2,1)} %wq_hbm.1, ...), custom_call_target="tpu_custom_call" | custom-call | tf_op jit(solution)/shard_map/attention/pallas_call | solution.py:212
  10.8 1.5 %collective-permute-start = (bf16[48,2048]{1,0:T(8,128)(2,1)S(1)}, bf16[48,2048]{1,0:T(8,128)(2,1)S(1)}, u32[]{:S(2)}, u32[]{:S(2)}) collective-permute-start(bf16[48,2048]{1,0:T(8,128)(2,1)S(1)} %get-tuple-element.16.own_ref), channel_id=1, source_target_pairs={{0,1},{1,0},{2,3},{3,2},{4,5},{5,4},{6,7},{7,6},{8,9},{9,8},{10,11... | collective-permute-start | bytes 589832 | tf_op jit(solution)/shard_map/ppermute | solution.py:426
  12.2 1.1 %collective-permute-done.peer_ref = bf16[48,2048]{1,0:T(8,128)(2,1)S(1)} collective-permute-done((bf16[48,2048]{1,0:T(8,128)(2,1)S(1)}, bf16[48,2048]{1,0:T(8,128)(2,1)S(1)}, u32[]{:S(2)}, u32[]{:S(2)}) %collective-permute-start) | collective-permute-done | bytes 196640 | tf_op jit(solution)/shard_map/ppermute | solution.py:426
  13.3 0.0 copy-done
  13.3 0.0 copy-done.1
  13.3 0.9 %dispatch.1 = (bf16[3072,128]{1,0:T(8,128)(2,1)S(1)}, bf16[48,2048]{1,0:T(8,128)(2,1)S(1)}) custom-call(bf16[48,2048]{1,0:T(8,128)(2,1)S(1)} %copy-done, bf16[48,2048]{1,0:T(8,128)(2,1)S(1)} %get-tuple-element.16.own_ref, bf16[48,2048]{1,0:T(8,128)(2,1)S(1)} %collective-permute-done.peer_ref, bf16[16,128]{1,0:T(8,128)(2,1)S(1)} %bitcast.21, ...), custom_call_target="tpu_custom_call" | custom-call | tf_op jit(solution)/shard_map/dispatch/pallas_call | solution.py:282
  14.2 0.5 collective-permute-start.1
  14.6 26.5 %all_to_all.10 = bf16[64,48,128]{2,1,0:T(8,128)(2,1)S(1)} all-to-all(bf16[64,48,128]{2,1,0:T(8,128)(2,1)S(1)} %bitcast.20), channel_id=1, replica_groups=mesh['ep'=64,'tp'=2] {'ep'}, dimensions={0} | all-to-all | bytes 1572864 | tf_op jit(solution)/shard_map/all_to_all | solution.py:433
  41.1 0.0 collective-permute-done.1.peer_ref
  41.1 2.0 %experts.1 = bf16[3072,128]{1,0:T(8,128)(2,1)S(1)} custom-call(bf16[3072,128]{1,0:T(8,128)(2,1)S(1)} %bitcast.18, bf16[6144,256]{1,0:T(8,128)(2,1)S(1)} %get-tuple-element.19.own_ref, bf16[6144,256]{1,0:T(8,128)(2,1)S(1)} %collective-permute-done.1.peer_ref), custom_call_target="tpu_custom_call" | custom-call | tf_op jit(solution)/shard_map/experts/pallas_call | solution.py:336
  43.2 18.1 %all_to_all.11 = bf16[64,48,128]{2,1,0:T(8,128)(2,1)S(1)} all-to-all(bf16[64,48,128]{2,1,0:T(8,128)(2,1)S(1)} %bitcast.19), channel_id=1, replica_groups=mesh['ep'=64,'tp'=2] {'ep'}, dimensions={0} | all-to-all | bytes 1572864 | tf_op jit(solution)/shard_map/all_to_all | solution.py:433
  61.3 1.0 %give.1 = bf16[48,1024]{1,0:T(8,128)(2,1)S(1)} custom-call(s32[1]{0:T(128)} %bitcast.core, f32[4,48]{1,0:T(4,128)S(1)} %get-tuple-element.13.shares_any, s32[8,48]{1,0:T(8,128)S(1)} %get-tuple-element.14.slots_any, bf16[3072,128]{1,0:T(8,128)(2,1)S(1)} %bitcast.16), custom_call_target="tpu_custom_call" | custom-call | tf_op jit(solution)/shard_map/give/pallas_call | solution.py:380
  62.3 3.2 %collective-permute-start.2 = (bf16[48,1024]{1,0:T(8,128)(2,1)S(1)}, bf16[48,1024]{1,0:T(8,128)(2,1)S(1)}, u32[]{:S(2)}, u32[]{:S(2)}) collective-permute-start(bf16[48,1024]{1,0:T(8,128)(2,1)S(1)} %give.1), channel_id=1, source_target_pairs={{0,1},{1,0},{2,3},{3,2},{4,5},{5,4},{6,7},{7,6},{8,9},{9,8},{10,11... | collective-permute-start | bytes 294920 | tf_op jit(solution)/shard_map/ppermute | solution.py:439
  65.5 1.1 %keep.1 = f32[48,1024]{1,0:T(8,128)S(1)} custom-call(s32[1]{0:T(128)} %bitcast.core, f32[4,48]{1,0:T(4,128)S(1)} %get-tuple-element.13.shares_any, s32[8,48]{1,0:T(8,128)S(1)} %get-tuple-element.14.slots_any, bf16[3072,128]{1,0:T(8,128)(2,1)S(1)} %bitcast.17, bf16[48,2048]{1,0:T(8,128)(2,1)S(1)} %get-tuple-element.20.refs_0_), custom_call_target="tpu_custom_call" | custom-call | tf_op jit(solution)/shard_map/keep/pallas_call | solution.py:380
  66.6 0.0 collective-permute-done.2
  66.6 0.7 add_convert_fusion
Async XLA Ops:
  0.0 13.3 %copy-start = (bf16[48,2048]{1,0:T(8,128)(2,1)S(1)}, bf16[48,2048]{1,0:T(8,128)(2,1)}, u32[]{:S(2)}) copy-start(bf16[48,2048]{1,0:T(8,128)(2,1)} %tokens_ref.1) | copy-start | bytes 589828
  0.0 13.3 %copy-start.1 = (bf16[2048]{0:T(1024)(128)(2,1)S(1)}, bf16[2048]{0:T(1024)(128)(2,1)}, u32[]{:S(2)}) copy-start(bf16[2048]{0:T(1024)(128)(2,1)} %param.19) | copy-start | bytes 12292
  10.8 2.5 %collective-permute-start = (bf16[48,2048]{1,0:T(8,128)(2,1)S(1)}, bf16[48,2048]{1,0:T(8,128)(2,1)S(1)}, u32[]{:S(2)}, u32[]{:S(2)}) collective-permute-start(bf16[48,2048]{1,0:T(8,128)(2,1)S(1)} %get-tuple-element.16.own_ref), channel_id=1, source_target_pairs={{0,1},{1,0},{2,3},{3,2},{4,5},{5,4},{6,7},{7,6},{8,9},{9,8},{10,11... | collective-permute-start | bytes 589832 | tf_op jit(solution)/shard_map/ppermute | solution.py:426
  14.2 27.0 %collective-permute-start.1 = (bf16[6144,256]{1,0:T(8,128)(2,1)S(1)}, bf16[6144,256]{1,0:T(8,128)(2,1)S(1)}, u32[]{:S(2)}, u32[]{:S(2)}) collective-permute-start(bf16[6144,256]{1,0:T(8,128)(2,1)S(1)} %get-tuple-element.19.own_ref), channel_id=1, source_target_pairs={{0,1},{1,0},{2,3},{3,2},{4,5},{5,4},{6,7},{7,6},{8,9},{9,8},{10,11... | collective-permute-start | bytes 9437192 | tf_op jit(solution)/shard_map/ppermute | solution.py:429
  62.3 4.3 %collective-permute-start.2 = (bf16[48,1024]{1,0:T(8,128)(2,1)S(1)}, bf16[48,1024]{1,0:T(8,128)(2,1)S(1)}, u32[]{:S(2)}, u32[]{:S(2)}) collective-permute-start(bf16[48,1024]{1,0:T(8,128)(2,1)S(1)} %give.1), channel_id=1, source_target_pairs={{0,1},{1,0},{2,3},{3,2},{4,5},{5,4},{6,7},{7,6},{8,9},{9,8},{10,11... | collective-permute-start | bytes 294920 | tf_op jit(solution)/shard_map/ppermute | solution.py:439
